TPU v7x, 512 devices: a whole 4x4x16 slice. The times are simulated.
512 devices in a mesh: sp: 64 (over z, y), tp: 8 (over x, core).
Axes of the slice: x: 4, y: 4, z: 16, core: 2. Of those that a mesh axis runs over, the one named last changes fastest.
Arguments:
- stream: bfloat16 [8192, 2048], P('sp'), may hold values from -6 to 6
- query_narrow: bfloat16 [8192, 512], P('sp', 'tp'), may hold values from -7 to 7
- query_broad: bfloat16 [8192, 1024], P('sp', 'tp'), may hold values from -7 to 7
- key_narrow: bfloat16 [8192, 512], P('sp', 'tp'), may hold values from -7 to 7
- key_broad: bfloat16 [8192, 1024], P('sp', 'tp'), may hold values from -7 to 7
- value_narrow: bfloat16 [8192, 512], P('sp', 'tp'), may hold values from -6 to 6
- value_broad: bfloat16 [8192, 1024], P('sp', 'tp'), may hold values from -6 to 6
- key_offsets: float32 [8192, 16], P('sp', 'tp'), may hold values from -20 to 0
- out_narrow: bfloat16 [512, 2048], P('tp'), may hold values from -0.4375 to 0.4375
- out_broad: bfloat16 [1024, 2048], P('tp'), may hold values from -0.4375 to 0.4375
- norm_gain: float32 [2048], replicated, may hold values from 0.1 to 1.9
- gate_weight: bfloat16 [2048, 3072], P('sp', 'tp'), may hold values from -0.125 to 0.125
- up_weight: bfloat16 [2048, 3072], P('sp', 'tp'), may hold values from -0.125 to 0.125
- down_weight: bfloat16 [3072, 2048], P('tp', 'sp'), may hold values from -0.21875 to 0.21875
Outputs:
- result: bfloat16 [8192, 2048], P(('sp', 'tp'))
All inputs are finite; a program needn't handle non-finite values.
Results may differ from a plain program's by a relative error of at most 0.028.
Values may be sent and summed in bfloat16 or wider, within the bound.
A program may use at most 64 MiB of HBM per device.

v0:
```python
import jax
import jax.numpy as jnp
from jax import lax
from jax.sharding import Mesh
from jax.sharding import PartitionSpec as P

NARROW_SIZE = 64
BROAD_SIZE = 128
SP = ("sp_0", "sp_1")
SP_TP = ("sp_0", "sp_1", "tp")


grain = 8
block_keys = 512
norm_eps = 1e-06


def laid_out(blocks, dim):
    blocks = jnp.moveaxis(blocks, 0, dim)
    shape = blocks.shape
    return blocks.reshape(*shape[:dim], shape[dim] * shape[dim + 1], *shape[dim + 2 :])


def gather_in_order(shard, axes, sequence):
    blocks = shard[None]
    for k in sequence:
        blocks = lax.all_gather(blocks, axes[k], axis=0, tiled=True)
    carried = [lax.axis_size(axes[k]) for k in reversed(sequence)]
    blocks = blocks.reshape(*carried, *shard.shape)
    turned = sorted(range(len(sequence)), key=lambda place: sequence[len(sequence) - 1 - place])
    return blocks.transpose(*turned, *range(len(sequence), blocks.ndim)).reshape(-1, *shard.shape)


def whole_of(shard, axes, sequence, dim):
    return laid_out(gather_in_order(shard, axes, sequence), dim)


def sent_to_all(shard, axis):
    peers = lax.axis_size(axis)
    return lax.all_to_all(
        jnp.broadcast_to(shard[None], (peers, *shard.shape)), axis, 0, 0, tiled=True
    )


def over_copies(shard, axis):
    return sent_to_all(shard, axis).astype(jnp.float32).sum(axis=0)


def in_one_piece(arrays, axis, dim, along):
    widths = [a.shape[along] for a in arrays]
    both = jnp.concatenate(arrays, axis=along)
    filled = lax.all_gather(both, axis, axis=dim, tiled=True)
    return tuple(jnp.split(filled, [sum(widths[:k]) for k in range(1, len(widths))], axis=along))


def gather_axes(shard, axes, dim):
    filled = shard
    for number in range(len(axes) - 1, -1, -1):
        filled = lax.all_gather(filled, axes[number], axis=dim, tiled=True)
    return filled


def cut_along(shard, dim, peers):
    shape = shard.shape
    blocks = shard.reshape(*shape[:dim], peers, shape[dim] // peers, *shape[dim + 1 :])
    return jnp.moveaxis(blocks, dim, 0)


def summed_on_arrival(shard, axis, dim):
    peers = lax.axis_size(axis)
    blocks = lax.all_to_all(cut_along(shard, dim, peers), axis, 0, 0, tiled=True)
    return jnp.sum(blocks.astype(jnp.float32), axis=0)


def block_plan(length):
    return (length // block_keys, block_keys)


def slice_rows(array, first, count):
    return lax.dynamic_slice_in_dim(array, first, count, 0)


def head_logs(queries, keys_block, offset_block, positions, key_positions, scale):
    logits = (
        jnp.einsum("qhd,khd->hqk", queries, keys_block, preferred_element_type=jnp.float32) * scale
    )
    logits = logits + jnp.transpose(offset_block)[:, None, :]
    causal = (key_positions[None, :] < positions[:, None])[None, :, :]
    lognot = jnp.where(causal, jax.nn.log_sigmoid(-logits), 0.0)
    return (logits, causal, lognot)


def sub_totals(lognot):
    heads, count, length = lognot.shape
    return lognot.reshape(heads, count, length // grain, grain).sum(axis=3)


def weighted_values(logits, causal, lognot, after, values):
    heads, count, length = lognot.shape
    grouped = lognot.reshape(heads, count, length // grain, grain)
    within = lax.cumsum(grouped, axis=3, reverse=True) - grouped
    later = (within + after[:, :, :, None]).reshape(heads, count, length)
    weights = jnp.where(causal, jnp.exp(jax.nn.log_sigmoid(logits) + later), 0.0).astype(
        jnp.bfloat16
    )
    return jnp.einsum("hqk,khd->qhd", weights, values, preferred_element_type=jnp.float32)


def local(
    stream,
    query_narrow,
    query_broad,
    key_narrow,
    key_broad,
    value_narrow,
    value_broad,
    key_offsets,
    out_narrow,
    out_broad,
    norm_gain,
    gate_weight,
    up_weight,
    down_weight,
):
    rows = stream.shape[0]
    heads = query_narrow.shape[1] // NARROW_SIZE
    shaped_narrow = query_narrow.reshape(rows, heads, NARROW_SIZE)
    shaped_broad = query_broad.reshape(rows, heads, BROAD_SIZE)
    positions = lax.axis_index(SP) * rows + jnp.arange(rows, dtype=jnp.int32)
    scale_narrow = NARROW_SIZE ** (-0.5)
    scale_broad = BROAD_SIZE ** (-0.5)

    def key_block(keys_narrow, keys_broad, offsets, first, count):
        block_narrow = slice_rows(keys_narrow, first, count).reshape(count, heads, NARROW_SIZE)
        block_broad = slice_rows(keys_broad, first, count).reshape(count, heads, BROAD_SIZE)
        pairs = slice_rows(offsets, first, count).reshape(count, heads, 2)
        return (block_narrow, block_broad, pairs[:, :, 0], pairs[:, :, 1])

    def value_block(values_narrow, values_broad, first, count):
        return (
            slice_rows(values_narrow, first, count).reshape(count, heads, NARROW_SIZE),
            slice_rows(values_broad, first, count).reshape(count, heads, BROAD_SIZE),
        )

    empty_narrow = jnp.zeros((rows, heads, NARROW_SIZE), jnp.float32)
    empty_broad = jnp.zeros((rows, heads, BROAD_SIZE), jnp.float32)
    whole = (
        whole_of(key_narrow, SP, (0, 1), 0),
        whole_of(key_broad, SP, (0, 1), 0),
        whole_of(value_narrow, SP, (0, 1), 0),
        whole_of(value_broad, SP, (0, 1), 0),
        whole_of(key_offsets.astype(jnp.bfloat16), SP, (0, 1), 0).astype(key_offsets.dtype),
    )
    keys_narrow, keys_broad, values_narrow, values_broad, offsets = whole
    steps, span = block_plan(keys_narrow.shape[0])
    running = jnp.zeros((heads, rows), jnp.float32)

    def back_step(index, state):
        first = (steps - 1 - index) * span
        block_narrow, block_broad, offset_narrow, offset_broad = key_block(
            keys_narrow, keys_broad, offsets, first, span
        )
        held_narrow, held_broad = value_block(values_narrow, values_broad, first, span)
        key_positions = first + jnp.arange(span, dtype=jnp.int32)
        logits_narrow, causal_narrow, lognot_narrow = head_logs(
            shaped_narrow, block_narrow, offset_narrow, positions, key_positions, scale_narrow
        )
        logits_broad, causal_broad, lognot_broad = head_logs(
            shaped_broad, block_broad, offset_broad, positions, key_positions, scale_broad
        )
        subs_narrow = sub_totals(lognot_narrow)
        subs_broad = sub_totals(lognot_broad)
        later_narrow = (
            lax.cumsum(subs_narrow, axis=2, reverse=True) - subs_narrow + state[2][:, :, None]
        )
        later_broad = (
            lax.cumsum(subs_broad, axis=2, reverse=True) - subs_broad + state[3][:, :, None]
        )
        return (
            state[0]
            + weighted_values(
                logits_narrow, causal_narrow, lognot_narrow, later_narrow, held_narrow
            ),
            state[1]
            + weighted_values(logits_broad, causal_broad, lognot_broad, later_broad, held_broad),
            state[2] + subs_narrow.sum(axis=2),
            state[3] + subs_broad.sum(axis=2),
        )

    final = lax.fori_loop(0, steps, back_step, (empty_narrow, empty_broad, running, running))
    acc_narrow = final[0]
    acc_broad = final[1]
    attended_narrow = acc_narrow.reshape(rows, heads * NARROW_SIZE).astype(jnp.bfloat16)
    attended_broad = acc_broad.reshape(rows, heads * BROAD_SIZE).astype(jnp.bfloat16)
    share = rows // lax.axis_size("tp")
    own = lax.axis_index("tp") * share
    summed = over_copies(
        (
            jnp.dot(
                slice_rows(attended_narrow, 0, rows), out_narrow, preferred_element_type=jnp.float32
            )
            + jnp.dot(
                slice_rows(attended_broad, 0, rows), out_broad, preferred_element_type=jnp.float32
            )
        ).astype(jnp.bfloat16),
        "tp",
    ).astype(jnp.float32)
    mid_all = (stream.astype(jnp.float32) + summed).astype(jnp.bfloat16)
    middle = mid_all.astype(jnp.float32)
    scaled = middle * lax.rsqrt(jnp.mean(middle * middle, axis=1, keepdims=True) + norm_eps)
    normed = (scaled * norm_gain).astype(jnp.bfloat16)
    mid_own = slice_rows(mid_all, own, share)
    part_gate, part_up = in_one_piece((gate_weight, up_weight), SP, 0, 1)
    gate = jnp.dot(normed, part_gate, preferred_element_type=jnp.float32)
    up = jnp.dot(normed, part_up, preferred_element_type=jnp.float32)
    hidden = (jax.nn.silu(gate) * up).astype(jnp.bfloat16)
    down_full = gather_axes(down_weight, SP, 1)
    mixed = summed_on_arrival(
        jnp.dot(
            slice_rows(hidden, jnp.int32(0), share * lax.axis_size("tp")),
            down_full,
            preferred_element_type=jnp.float32,
        ).astype(jnp.bfloat16),
        "tp",
        0,
    )
    return (mid_own.astype(jnp.float32) + mixed).astype(jnp.bfloat16)


def solution(mesh):
    torus = Mesh(mesh.devices.reshape(16, 4, mesh.shape["tp"]), ("sp_0", "sp_1", "tp"))
    in_specs = (
        P(SP, None),
        P(SP, "tp"),
        P(SP, "tp"),
        P(SP, "tp"),
        P(SP, "tp"),
        P(SP, "tp"),
        P(SP, "tp"),
        P(SP, "tp"),
        P("tp", None),
        P("tp", None),
        P(),
        P(SP, "tp"),
        P(SP, "tp"),
        P("tp", SP),
    )
    out_specs = P(SP_TP, None)
    return jax.shard_map(local, mesh=torus, in_specs=in_specs, out_specs=out_specs, check_vma=False)
```

profile of v0, /device:TPU:1, one launch (start us, length us, event | category | flops | bytes accessed | tf_op | source)
XLA Modules:
  0.0 433.5 jit_solution(11852103382589410577)
XLA Ops:
  6.6 30.8 %all-gather = bf16[2048,64]{0,1:T(8,128)(2,1)S(1)} all-gather(bf16[128,64]{0,1:T(8,128)(2,1)} %param.21), channel_id=2, replica_groups=mesh['sp_0'=16,'sp_1'=4,'tp'=8] {'sp_0'}, dimensions={0}, use_global_device_ids=true | all-gather | bytes 278528 | tf_op jit(solution)/shard_map/all_gather | solution.py:27
  38.2 21.0 %all-gather.1 = bf16[2048,64]{0,1:T(8,128)(2,1)S(1)} all-gather(bf16[128,64]{0,1:T(8,128)(2,1)} %param.19), channel_id=3, replica_groups=mesh['sp_0'=16,'sp_1'=4,'tp'=8] {'sp_0'}, dimensions={0}, use_global_device_ids=true | all-gather | bytes 278528 | tf_op jit(solution)/shard_map/all_gather | solution.py:27
  60.1 26.6 %all-gather.3 = bf16[2048,128]{1,0:T(8,128)(2,1)} all-gather(bf16[128,128]{1,0:T(8,128)(2,1)S(1)} %copy-done.4), channel_id=5, replica_groups=mesh['sp_0'=16,'sp_1'=4,'tp'=8] {'sp_0'}, dimensions={0}, use_global_device_ids=true | all-gather | bytes 557056 | tf_op jit(solution)/shard_map/all_gather | solution.py:27
  86.7 25.8 %all-gather.4 = bf16[2048,128]{1,0:T(8,128)(2,1)} all-gather(bf16[128,128]{1,0:T(8,128)(2,1)S(1)} %copy-done.5), channel_id=6, replica_groups=mesh['sp_0'=16,'sp_1'=4,'tp'=8] {'sp_0'}, dimensions={0}, use_global_device_ids=true | all-gather | bytes 557056 | tf_op jit(solution)/shard_map/all_gather | solution.py:27
  113.4 19.6 %all-gather.2 = bf16[2048,2]{0,1:T(2,128)(2,1)S(1)} all-gather(bf16[128,2]{0,1:T(2,128)(2,1)S(1)} %convert_element_type.77), channel_id=4, replica_groups=mesh['sp_0'=16,'sp_1'=4,'tp'=8] {'sp_0'}, dimensions={0}, use_global_device_ids=true | all-gather | bytes 8704 | tf_op jit(solution)/shard_map/all_gather | solution.py:27
  132.9 12.1 %all_gather.44 = bf16[64,128,2]{1,0,2:T(8,128)(2,1)S(1)} all-gather(bf16[16,128,2]{1,0,2:T(8,128)(2,1)S(1)} %bitcast.157), channel_id=1, replica_groups=mesh['sp_0'=16,'sp_1'=4,'tp'=8] {'sp_1'}, dimensions={0}, use_global_device_ids=true | all-gather | bytes 40960 | tf_op jit(solution)/shard_map/all_gather | solution.py:27
  145.1 3.1 copy.44
  148.3 3.1 copy.46
  152.4 3.2 copy.39
  155.6 37.4 %all-gather.18.cloned.1.call-done = bf16[64,128,128]{2,1,0:T(8,128)(2,1)} async-done(((bf16[16,128,128]{2,1,0:T(8,128)(2,1)}), bf16[64,128,128]{2,1,0:T(8,128)(2,1)}) %all-gather.18.cloned.1.call-update) | async-done | bytes 2097168 | tf_op jit(solution)/shard_map/all_gather | solution.py:27
  193.0 3.3 copy.40
  196.3 116.7 %while.20 = (s32[]{:T(128)}, f32[128,1,64]{0,2,1:T(8,128)S(1)}, f32[128,1,128]{0,2,1:T(8,128)S(1)}, f32[1,128]{1,0:T(1,128)S(1)}, f32[1,128]{1,0:T(1,128)S(1)}, ...) while((s32[]{:T(128)}, f32[128,1,64]{0,2,1:T(8,128)S(1)}, ...), condition=%wide.region_9.10_spmd.clone, body=%wide.region_0.9_spmd.clone.sunk | while | flops 57983880 | bytes 5200671 | solution.py:190
  200.0 1.5 fusion.94
  207.3 1.5 fusion.94
  209.4 1.4 fusion.93
  214.6 1.5 fusion.94
  216.7 1.4 fusion.93
  221.8 1.5 fusion.94
  224.0 1.4 fusion.93
  229.1 1.5 fusion.94
  236.4 1.5 fusion.94
  238.6 1.4 fusion.93
  243.7 1.5 fusion.94
  251.0 1.5 fusion.94
  258.3 1.5 fusion.94
  260.5 1.4 fusion.93
  265.6 1.5 fusion.94
  272.9 1.5 fusion.94
  275.1 1.4 fusion.93
  280.2 1.5 fusion.94
  282.4 1.4 fusion.93
  287.5 1.5 fusion.94
  294.8 1.5 fusion.94
  297.0 1.4 fusion.93
  302.1 1.5 fusion.94
  304.3 1.4 fusion.93
  309.4 1.5 fusion.94
  311.6 1.4 fusion.93
  313.7 2.5 broadcast_in_dim.69
  316.2 5.4 %all-to-all-start = ((bf16[8,128,2048]{2,1,0:T(8,128)(2,1)}), bf16[8,128,2048]{2,1,0:T(8,128)(2,1)}, u32[]{:S(2)}, u32[]{:S(2)}) async-start(bf16[8,128,2048]{2,1,0:T(8,128)(2,1)} %broadcast_in_dim.69), calls=%async_computation | async-start | bytes 8388608 | tf_op jit(solution)/shard_map/all_to_all | solution.py:40
  321.6 10.7 %all_gather.50 = bf16[384,128]{0,1:T(8,128)(2,1)} all-gather(bf16[384,32]{0,1:T(8,128)(2,1)S(1)} %copy-done.8), channel_id=1, replica_groups=mesh['sp_0'=16,'sp_1'=4,'tp'=8] {'sp_1'}, dimensions={1}, use_global_device_ids=true | all-gather | bytes 122880 | tf_op jit(solution)/shard_map/all_gather | solution.py:59
  332.3 38.1 %all-to-all-done = bf16[8,128,2048]{2,1,0:T(8,128)(2,1)} async-done(((bf16[8,128,2048]{2,1,0:T(8,128)(2,1)}), bf16[8,128,2048]{2,1,0:T(8,128)(2,1)}, u32[]{:S(2)}, u32[]{:S(2)}) %all-to-all-start) | async-done | bytes 4194336 | tf_op jit(solution)/shard_map/all_to_all | solution.py:40
  370.4 3.0 convert_reduce_fusion
  374.1 1.9 fusion.41
  376.0 23.2 %all-gather.22.cloned.1.call-done = bf16[384,2048]{0,1:T(8,128)(2,1)} async-done(((bf16[384,128]{0,1:T(8,128)(2,1)}), bf16[384,2048]{0,1:T(8,128)(2,1)}) %all-gather.22.cloned.1.call-update) | async-done | bytes 1572880 | tf_op jit(solution)/shard_map/all_gather | solution.py:59
  399.3 3.7 convolution_convert_fusion
  403.0 13.6 %all-to-all-start.1 = ((bf16[8,16,2048]{2,1,0:T(8,128)(2,1)}), bf16[8,16,2048]{2,1,0:T(8,128)(2,1)S(1)}, u32[]{:S(2)}, u32[]{:S(2)}) async-start(bf16[8,16,2048]{2,1,0:T(8,128)(2,1)} %bitcast.22), calls=%async_computation.1 | async-start | bytes 1048576 | tf_op jit(solution)/shard_map/all_to_all | solution.py:71
  416.6 9.3 %all-to-all-done.1 = bf16[8,16,2048]{2,1,0:T(8,128)(2,1)S(1)} async-done(((bf16[8,16,2048]{2,1,0:T(8,128)(2,1)}), bf16[8,16,2048]{2,1,0:T(8,128)(2,1)S(1)}, u32[]{:S(2)}, u32[]{:S(2)}) %all-to-all-start.1) | async-done | bytes 524320 | tf_op jit(solution)/shard_map/all_to_all | solution.py:71
  (288 shorter events, 82.8 us)
Async XLA Ops:
  6.5 306.8 %copy-start = (bf16[128,2048]{1,0:T(8,128)(2,1)S(1)}, bf16[128,2048]{1,0:T(8,128)(2,1)}, u32[]{:S(2)}) copy-start(bf16[128,2048]{1,0:T(8,128)(2,1)} %param.25) | copy-start | bytes 1572868
  6.5 53.5 %copy-start.4 = (bf16[128,128]{1,0:T(8,128)(2,1)S(1)}, bf16[128,128]{1,0:T(8,128)(2,1)}, u32[]{:S(2)}) copy-start(bf16[128,128]{1,0:T(8,128)(2,1)} %param.22) | copy-start | bytes 98308
  6.5 80.2 %copy-start.5 = (bf16[128,128]{1,0:T(8,128)(2,1)S(1)}, bf16[128,128]{1,0:T(8,128)(2,1)}, u32[]{:S(2)}) copy-start(bf16[128,128]{1,0:T(8,128)(2,1)} %param.20) | copy-start | bytes 98308
  6.5 106.1 %copy-start.7 = (bf16[32,384]{1,0:T(8,128)(2,1)S(1)}, bf16[32,384]{1,0:T(8,128)(2,1)}, u32[]{:S(2)}) copy-start(bf16[32,384]{1,0:T(8,128)(2,1)} %param.27) | copy-start | bytes 73732
  6.5 106.1 %copy-start.6 = (bf16[32,384]{1,0:T(8,128)(2,1)S(1)}, bf16[32,384]{1,0:T(8,128)(2,1)}, u32[]{:S(2)}) copy-start(bf16[32,384]{1,0:T(8,128)(2,1)} %param.28) | copy-start | bytes 73732
  6.5 138.6 %all-gather.12.cloned.1.call-start = ((), (), s32[]{:S(2)}) async-start(), calls=%async_computation.2 | async-start | bytes 1310720 | tf_op jit(solution)/shard_map/all_gather | solution.py:27
  37.4 75.9 %copy-start.11 = (f32[128,2]{0,1:T(2,128)S(1)}, f32[128,2]{0,1:T(2,128)}, u32[]{:S(2)}) copy-start(f32[128,2]{0,1:T(2,128)} %param.23) | copy-start | bytes 3076
  38.2 110.1 %all-gather.14.cloned.1.call-start = ((), (), s32[]{:S(2)}) async-start(), calls=%async_computation.3 | async-start | bytes 1310720 | tf_op jit(solution)/shard_map/all_gather | solution.py:27
  60.0 92.4 %all-gather.16.cloned.1.call-start = ((), (), s32[]{:S(2)}) async-start(), calls=%async_computation.4 | async-start | bytes 2621440 | tf_op jit(solution)/shard_map/all_gather | solution.py:27
  86.6 106.3 %all-gather.18.cloned.1.call-start = ((), (), s32[]{:S(2)}) async-start(), calls=%async_computation.5 | async-start | bytes 2621440 | tf_op jit(solution)/shard_map/all_gather | solution.py:27
  112.6 261.2 %all-gather.20.cloned.1.call-start = ((), (), s32[]{:S(2)}) async-start(), calls=%async_computation.6 | async-start | bytes 3194880 | tf_op jit(solution)/shard_map/all_gather | solution.py:52
  193.0 3.3 copy-start.2
  193.0 3.3 copy-start.9
  196.3 116.7 %copy-start.3 = (bf16[64,2048]{1,0:T(8,128)(2,1)S(1)}, bf16[64,2048]{1,0:T(8,128)(2,1)}, u32[]{:S(2)}) copy-start(bf16[64,2048]{1,0:T(8,128)(2,1)} %param.24) | copy-start | bytes 786436
  316.2 5.4 %copy-start.8 = (bf16[384,32]{0,1:T(8,128)(2,1)S(1)}, bf16[384,32]{0,1:T(8,128)(2,1)}, u32[]{:S(2)}) copy-start(bf16[384,32]{0,1:T(8,128)(2,1)} %param.29) | copy-start | bytes 73732
  316.2 54.2 %all-to-all-start = ((bf16[8,128,2048]{2,1,0:T(8,128)(2,1)}), bf16[8,128,2048]{2,1,0:T(8,128)(2,1)}, u32[]{:S(2)}, u32[]{:S(2)}) async-start(bf16[8,128,2048]{2,1,0:T(8,128)(2,1)} %broadcast_in_dim.69), calls=%async_computation | async-start | bytes 8388608 | tf_op jit(solution)/shard_map/all_to_all | solution.py:40
  321.6 77.7 %all-gather.22.cloned.1.call-start = ((), (), s32[]{:S(2)}) async-start(), calls=%async_computation.7 | async-start | bytes 1671168 | tf_op jit(solution)/shard_map/all_gather | solution.py:59
  332.3 41.1 %copy-start.1 = (bf16[128,2048]{1,0:T(8,128)(2,1)S(1)}, bf16[128,2048]{1,0:T(8,128)(2,1)}, u32[]{:S(2)}) copy-start(bf16[128,2048]{1,0:T(8,128)(2,1)} %param.16) | copy-start | bytes 1572868
  373.4 0.7 copy-start.10
  403.0 23.0 %all-to-all-start.1 = ((bf16[8,16,2048]{2,1,0:T(8,128)(2,1)}), bf16[8,16,2048]{2,1,0:T(8,128)(2,1)S(1)}, u32[]{:S(2)}, u32[]{:S(2)}) async-start(bf16[8,16,2048]{2,1,0:T(8,128)(2,1)} %bitcast.22), calls=%async_computation.1 | async-start | bytes 1048576 | tf_op jit(solution)/shard_map/all_to_all | solution.py:71
Sparse Core Ops, SparseCore 0:
  38.3 34.8 all-gather.11
  75.3 33.8 all-gather.13
  111.3 41.0 all-gather.15
  154.4 38.5 all-gather.17
  195.8 134.4 all-gather.19
  332.4 66.7 all-gather.21
where the time goes:
time: 435 us; the launch traced here: 434 us
  blocking collectives  146 us (34%)
  waiting for transfers between devices  109 us (25%)
  matrix products  93 us (21%)
  other arithmetic  32.7 us (8%)
  starting transfers between devices  19.2 us (4%)
  local copies, waits for them, and re-layouts  17.6 us (4%)
  between operations  13.7 us (3%)
    all_gather x6, blocking collectives, gather_in_order(): blocks = lax.all_gather(blocks, axes[k], axis=0, tiled=True)  136 us
    dot_general x32, matrix products, weighted_values(): jnp.einsum('hqk,khd->qhd', weights, values, preferred_element_type=jnp.fl...  46.6 us
    dot_general x32, matrix products, head_logs(): jnp.einsum('qhd,khd->hqk', queries, keys_block, preferred_element_type=jn...  40.1 us
    all_gather x4, waiting for transfers between devices, gather_in_order(): blocks = lax.all_gather(blocks, axes[k], axis=0, tiled=True)  38.4 us
    all_to_all x1, waiting for transfers between devices, sent_to_all(): lax.all_to_all(jnp.broadcast_to(shard[None], (peers, *shard.shape)), axis...  38.1 us
    all_gather x1, waiting for transfers between devices, gather_axes(): filled = lax.all_gather(filled, axes[number], axis=dim, tiled=True)  23.2 us
    all_to_all x1, starting transfers between devices, summed_on_arrival(): lax.all_to_all(cut_along(shard, dim, peers), axis, 0, 0, tiled=True)  13.6 us
    another operation x32, other arithmetic, weighted_values(): within = lax.cumsum(grouped, axis=3, reverse=True) - grouped  12.2 us
  transfers between devices with their start and end apart: 8, of which 5 were waited for; matrix products, arithmetic and copies ran while one was open for 32% of the time, Pallas kernels for 0%

commit v1 on v0

v1 whole, which is shorter than its diff:
```python
import functools
import math

import jax
import jax.numpy as jnp
from jax import lax
from jax.experimental import pallas as pl
from jax.experimental.pallas import tpu as pltpu
from jax.sharding import Mesh
from jax.sharding import PartitionSpec as P

NARROW_SIZE = 64
BROAD_SIZE = 128
SP = ("sp_0", "sp_1")
SP_TP = ("sp_0", "sp_1", "tp")
MESH = pl.DeviceIdType.MESH
LOG2E = 1.4426950408889634
SCALE = (NARROW_SIZE**-0.5 * LOG2E, BROAD_SIZE**-0.5 * LOG2E)
norm_eps = 1e-06
F32 = jnp.float32
BF16 = jnp.bfloat16
NT = (((1,), (1,)), ((), ()))
NN = (((1,), (0,)), ((), ()))


def dot(a, b, dims=NN, precision=None):
    return lax.dot_general(a, b, dims, preferred_element_type=F32, precision=precision)


def wrap(value, size):
    return lax.rem(value + 2 * size, size)


def layer_kernel(
    nz, ny, nt, rows, wrows, share,
    kv_in, off_in, q_in, gu_in, dt_in, stream_in, on_in, ob_in, gain_in,
    out,
    kv, off, qs, w, db, ow, st, gain, obuf, tall, ar, ao, part, rs, nb, mid_s, part2, rs2, hid,
    lsem, kvs, kvr, offs, offr, ws, wr, ds_, dr, q_s, q_r, dts, dtr, yas, yar, yrs, yrr,
    t_s, t_r, a_s, a_r, r1s, r1r, n_s, n_r, r2s, r2r,
):
    z = lax.axis_index("sp_0")
    y = lax.axis_index("sp_1")
    t = lax.axis_index("tp")
    up = (wrap(z + 1, nz), y, t)
    dn = (wrap(z - 1, nz), y, t)
    yp = (z, wrap(y + 1, ny), t)
    ym = (z, wrap(y - 1, ny), t)
    half = nz // 2

    def ypeer(j):
        return (z, wrap(y + j, ny), t)

    def tpeer(j):
        return (z, y, wrap(t + j, nt))

    def rc(src, dst, ssem, rsem, dev):
        return pltpu.make_async_remote_copy(
            src_ref=src, dst_ref=dst, send_sem=ssem, recv_sem=rsem,
            device_id=dev, device_id_type=MESH,
        )

    first = [
        pltpu.make_async_copy(kv_in, kv.at[z], lsem.at[0]),
        pltpu.make_async_copy(off_in, off.at[z], lsem.at[1]),
        pltpu.make_async_copy(q_in, qs.at[y], lsem.at[2]),
        pltpu.make_async_copy(gu_in, w.at[z, y], lsem.at[3]),
        pltpu.make_async_copy(dt_in, db.at[z, y], lsem.at[4]),
    ]
    second = [
        pltpu.make_async_copy(stream_in.at[pl.ds(t * share, share), :], st, lsem.at[5]),
        pltpu.make_async_copy(on_in, ow.at[pl.ds(64, 64), :], lsem.at[6]),
        pltpu.make_async_copy(ob_in, ow.at[pl.ds(128, 128), :], lsem.at[7]),
        pltpu.make_async_copy(gain_in, gain, lsem.at[8]),
    ]
    for c in first:
        c.start()
    for c in second:
        c.start()

    barrier = pltpu.get_barrier_semaphore()
    peers = [up, dn] + [ypeer(j) for j in range(1, ny)] + [tpeer(j) for j in range(1, nt)]
    for p in peers:
        pl.semaphore_signal(barrier, inc=1, device_id=p, device_id_type=MESH)

    ow[pl.ds(0, 64), :] = jnp.zeros((64, ow.shape[1]), BF16)
    tall[y] = jnp.zeros(tall.shape[1:], F32)

    def zero_body(i, carry):
        obuf[i] = jnp.zeros(obuf.shape[1:], F32)
        return carry

    lax.fori_loop(0, nz, zero_body, 0)
    for c in first:
        c.wait()
    pl.semaphore_wait(barrier, len(peers))

    def ring(buf, ssem, rsem, d, k, sub=None):
        zz = wrap(z - k + 1, nz) if d == 0 else wrap(z + k - 1, nz)
        ref = buf.at[zz] if sub is None else buf.at[zz, sub]
        return rc(ref, ref, ssem.at[d, k], rsem.at[d, k], up if d == 0 else dn)

    def kv_ring(d, k):
        return ring(kv, kvs, kvr, d, k)

    def off_ring(d, k):
        return ring(off, offs, offr, d, k)

    def w_ring(d, k):
        return ring(w, ws, wr, d, k, y)

    def d_ring(d, k):
        return ring(db, ds_, dr, d, k)

    def shard_z(d, k):
        return wrap(z - k, nz) if d == 0 else wrap(z + k, nz)

    def w_y(d, k, e):
        ref = w.at[shard_z(d, k), y]
        return rc(ref, ref, yas.at[d, k, e], yar.at[d, k, e], yp if e == 0 else ym)

    def w_relay(d, k):
        src_y = wrap(y - 1, ny) if d == 0 else wrap(y + 1, ny)
        ref = w.at[shard_z(d, k), src_y]
        return rc(ref, ref, yrs.at[d, k], yrr.at[d, k], yp if d == 0 else ym)

    def q_send(j):
        return rc(qs.at[y], qs.at[y], q_s.at[j], q_r.at[j], ypeer(j))

    def dt_send(j):
        return rc(db.at[z, y], db.at[z, y], dts.at[j], dtr.at[j], ypeer(j))

    def t_send(g, j):
        ref = tall.at[y, g]
        return rc(ref, ref, t_s.at[g, j], t_r.at[g, j], ypeer(j))

    for j in range(1, ny):
        q_send(j).start()
    for d in range(2):
        kv_ring(d, 1).start()
        off_ring(d, 1).start()
    for d in range(2):
        w_ring(d, 1).start()
    for j in range(1, ny):
        dt_send(j).start()
    for e in range(2):
        w_y(0, 0, e).start()

    key_row = lax.broadcasted_iota(jnp.int32, (rows, rows), 0)
    key_col = lax.broadcasted_iota(jnp.int32, (rows, rows), 1)
    tri = jnp.where(key_row > key_col, 1.0, 0.0).astype(BF16)
    sub_row = lax.broadcasted_iota(jnp.int32, (8, rows), 0)

    def process(zz, s, diag):
        def row_block(rb, carry):
            total = None
            for h in range(2):
                q = qs[rb, pl.ds(h * rows, rows), :]
                k = kv[zz, pl.ds(h * rows, rows), :]
                v = kv[zz, pl.ds(2 * h * rows, rows), :]
                logits = dot(q, k, NT) * SCALE[h] + off[zz, pl.ds(h, 1), :]
                soft = jnp.maximum(
                    jnp.log2(1.0 + jnp.exp2(jnp.minimum(logits, 126.0))), logits
                )
                if diag:
                    causal = (y * rows + key_col) < (rb * rows + key_row)
                    low = jnp.where(causal, soft, 0.0).astype(BF16)
                else:
                    low = soft.astype(BF16)
                after = dot(low, tri)
                weight = jnp.exp2(logits - soft - after)
                if diag:
                    weight = jnp.where(causal, weight, 0.0)
                obuf[s, h, pl.ds(rb * rows, rows), :] = dot(weight.astype(BF16), v)
                pick = jnp.where(sub_row == 2 * lax.rem(s, 4) + h, 1.0, 0.0).astype(BF16)
                mine = dot(pick, low, NT)
                total = mine if total is None else total + mine
            place = pl.ds(pl.multiple_of(rb * rows, rows), rows)
            g = lax.div(s, 4)
            tall[y, g, :, place] = tall[y, g, :, place] + total
            return carry

        lax.fori_loop(0, ny, row_block, 0)

    for j in range(1, ny):
        q_send(j).wait_recv()
    process(z, jnp.int32(0), True)

    def step(k, last):
        dirs = (0,) if last else (0, 1)
        for d in dirs:
            kv_ring(d, k).wait_recv()
            off_ring(d, k).wait_recv()
            if not last:
                if d == 0:
                    kv_ring(0, k + 1).start()
                    off_ring(0, k + 1).start()
                else:
                    @pl.when(k < half - 1)
                    def _():
                        kv_ring(1, k + 1).start()
                        off_ring(1, k + 1).start()
        for d in dirs:
            w_ring(d, k).wait_recv()
            if not last:
                if d == 0:
                    w_ring(0, k + 1).start()
                else:
                    @pl.when(k < half - 1)
                    def _():
                        w_ring(1, k + 1).start()
            for e in range(2):
                w_y(d, k, e).start()
        w_y(0, k - 1, 0).wait_recv()
        w_relay(0, k - 1).start()

        @pl.when(k >= 2)
        def _():
            w_y(1, k - 1, 1).wait_recv()
            w_relay(1, k - 1).start()

        @pl.when(k <= z)
        def _():
            process(wrap(z - k, nz), 2 * k - 1, False)

        if not last:
            @pl.when(z + k >= nz)
            def _():
                process(wrap(z + k, nz), 2 * k, False)

        @pl.when(lax.rem(k, 2) == 0)
        def _():
            for j in range(1, ny):
                t_send(lax.div(k, 2) - 1, j).start()

    def step_body(k, carry):
        step(k, False)
        return carry

    lax.fori_loop(1, half, step_body, 0)
    step(jnp.int32(half), True)

    for j in range(1, ny):
        dt_send(j).wait_recv()
    d_ring(0, 1).start()
    d_ring(1, 1).start()

    def d_step(k):
        if k > half:
            return
        d_ring(0, k).wait_recv()
        if k < half:
            d_ring(0, k + 1).start()
        if k < half:
            d_ring(1, k).wait_recv()
            if k < half - 1:
                d_ring(1, k + 1).start()

    w_y(0, half, 0).wait_recv()
    w_relay(0, half).start()

    ngroup = nz // 4
    for g in range(ngroup):
        for j in range(1, ny):
            t_send(g, j).wait_recv()
    d_step(1)

    trows = ny * ngroup * 8
    flat = tall[...].reshape(trows, ny * rows)
    fr = lax.broadcasted_iota(jnp.int32, (128, trows), 0)
    fc = lax.broadcasted_iota(jnp.int32, (128, trows), 1)

    def slot_z(slot):
        k = lax.shift_right_logical(slot + 1, 1)
        signed = jnp.where(lax.bitwise_and(slot, 1) == 1, -k, k)
        return lax.bitwise_and(z + signed + nz, nz - 1)

    per_y = ngroup * 8
    c_y = lax.div(fc, per_y)
    c_in = lax.rem(fc, per_y)
    r_order = slot_z(lax.shift_right_logical(fr, 1)) * ny + y
    c_order = slot_z(lax.shift_right_logical(c_in, 1)) * ny + c_y
    same = lax.bitwise_and(fr, 1) == lax.bitwise_and(c_in, 1)
    sel = jnp.where(jnp.logical_and(same, c_order > r_order), 1.0, 0.0).astype(F32)
    later = dot(sel, flat, NN, lax.Precision.HIGHEST)
    factor = jnp.exp2(-later)
    for rb in range(ny):
        ft = jnp.transpose(factor[:, rb * rows : (rb + 1) * rows])
        for h in range(2):
            acc = jnp.zeros((rows, 128), F32)
            for s in range(nz):
                col = lax.slice(ft, (0, 2 * s + h), (rows, 2 * s + h + 1))
                acc = acc + col * obuf[s, h, rb * rows : (rb + 1) * rows, :]
            ao[rb, :, h * 128 : (h + 1) * 128] = acc.astype(BF16)

    def a_send(j):
        peer = wrap(y + j, ny)
        return rc(ao.at[peer], ar.at[j], a_s.at[j], a_r.at[j], ypeer(j))

    for j in range(1, ny):
        a_send(j).start()
    d_step(2)
    d_step(3)
    for c in second:
        c.wait()
    attended = ao[y].astype(F32)
    for j in range(1, ny):
        a_send(j).wait_recv()
        attended = attended + ar[j].astype(F32)
    attended = attended.astype(BF16)
    model = out.shape[1]
    for c in range(model // 512):
        block = dot(attended, ow[:, c * 512 : (c + 1) * 512]).astype(BF16)
        part[:, :, c * 512 : (c + 1) * 512] = block.reshape(nt, share, 512)

    def r1_send(j):
        return rc(part.at[wrap(t + j, nt)], rs.at[j], r1s.at[j], r1r.at[j], tpeer(j))

    for j in range(1, nt):
        r1_send(j).start()
    d_step(4)
    d_step(5)
    total = st[...].astype(F32) + part[t].astype(F32)
    for j in range(1, nt):
        r1_send(j).wait_recv()
        total = total + rs[j].astype(F32)
    mid = total.astype(BF16).astype(F32)
    mid_s[...] = mid
    normed = mid * lax.rsqrt(jnp.mean(mid * mid, axis=1, keepdims=True) + norm_eps) * gain[...]
    nb[t] = normed.astype(BF16)

    def n_send(j):
        return rc(nb.at[t], nb.at[t], n_s.at[j], n_r.at[j], tpeer(j))

    for j in range(1, nt):
        n_send(j).start()
    for k in range(6, half + 1):
        d_step(k)

    def w_wait(k, d):
        if d == 0:
            w_y(0, k, 1).wait_recv()
            w_relay(0, k).wait_recv()
        else:
            w_y(1, k, 0).wait_recv()
            w_relay(1, k).wait_recv()

    def w_wait_body(k, carry):
        w_wait(k, 0)

        @pl.when(jnp.logical_and(k >= 1, k < half))
        def _():
            w_wait(k, 1)

        return carry

    lax.fori_loop(0, half + 1, w_wait_body, 0)
    for j in range(1, nt):
        n_send(j).wait_recv()

    gate = jnp.zeros((rows, w.shape[3]), F32)
    upv = jnp.zeros((rows, w.shape[3]), F32)
    span = ny * wrows
    for zz in range(nz):
        lhs = nb[:, :, zz * span : (zz + 1) * span].reshape(rows, span)
        gate = gate + dot(lhs, w[zz, :, 0:wrows, :].reshape(span, w.shape[3]))
        upv = upv + dot(lhs, w[zz, :, wrows : 2 * wrows, :].reshape(span, w.shape[3]))
    hidden = (gate / (1.0 + jnp.exp(-gate)) * upv).astype(BF16)
    for zz in range(nz):
        rhs = db[zz].reshape(span, db.shape[3])
        block = dot(hidden, rhs, NT).astype(BF16)
        part2[:, :, zz * span : (zz + 1) * span] = block.reshape(nt, share, span)

    def r2_send(j):
        return rc(part2.at[wrap(t + j, nt)], rs2.at[j], r2s.at[j], r2r.at[j], tpeer(j))

    for j in range(1, nt):
        r2_send(j).start()

    def drain(k, carry):
        for d in range(2):
            @pl.when(k <= half - d)
            def _():
                kv_ring(d, k).wait_send()
                off_ring(d, k).wait_send()
                w_ring(d, k).wait_send()
                d_ring(d, k).wait_send()
                for e in range(2):
                    w_y(d, k, e).wait_send()
                w_relay(d, k).wait_send()
        return carry

    lax.fori_loop(1, half + 1, drain, 0)
    for e in range(2):
        w_y(0, 0, e).wait_send()
    w_relay(0, 0).wait_send()
    for j in range(1, ny):
        q_send(j).wait_send()
        dt_send(j).wait_send()
        a_send(j).wait_send()
        for g in range(ngroup):
            t_send(g, j).wait_send()
    for j in range(1, nt):
        r1_send(j).wait_send()
        n_send(j).wait_send()
    total = mid_s[...] + part2[t].astype(F32)
    for j in range(1, nt):
        r2_send(j).wait_recv()
        total = total + rs2[j].astype(F32)
    out[...] = total.astype(BF16)
    for j in range(1, nt):
        r2_send(j).wait_send()


def local(
    nz, ny, nt,
    stream, query_narrow, query_broad, key_narrow, key_broad, value_narrow, value_broad,
    key_offsets, out_narrow, out_broad, norm_gain, gate_weight, up_weight, down_weight,
):
    rows, model = stream.shape
    wrows, ff = gate_weight.shape
    share = rows // nt
    half = nz // 2
    ngroup = nz // 4
    kv = jnp.concatenate(
        [jnp.concatenate([key_narrow, value_narrow], axis=1), key_broad, value_broad], axis=0
    )
    q = jnp.concatenate([jnp.pad(query_narrow, ((0, 0), (0, 64))), query_broad], axis=0)
    off = jnp.pad(jnp.transpose(key_offsets) * LOG2E, ((0, 6), (0, 0)))
    gu = jnp.concatenate([gate_weight, up_weight], axis=0)
    dt = jnp.transpose(down_weight)
    gain = norm_gain.reshape(1, model)
    dma = pltpu.SemaphoreType.DMA
    scratch = [
        pltpu.VMEM((nz, 3 * rows, 128), BF16),
        pltpu.VMEM((nz, 8, rows), F32),
        pltpu.VMEM((ny, 2 * rows, 128), BF16),
        pltpu.VMEM((nz, ny, 2 * wrows, ff), BF16),
        pltpu.VMEM((nz, ny, wrows, ff), BF16),
        pltpu.VMEM((256, model), BF16),
        pltpu.VMEM((share, model), BF16),
        pltpu.VMEM((1, model), F32),
        pltpu.VMEM((nz, 2, ny * rows, 128), F32),
        pltpu.VMEM((ny, ngroup, 8, ny * rows), F32),
        pltpu.VMEM((ny, rows, 256), BF16),
        pltpu.VMEM((ny, rows, 256), BF16),
        pltpu.VMEM((nt, share, model), BF16),
        pltpu.VMEM((nt, share, model), BF16),
        pltpu.VMEM((nt, share, model), BF16),
        pltpu.VMEM((share, model), F32),
        pltpu.VMEM((nt, share, model), BF16),
        pltpu.VMEM((nt, share, model), BF16),
        pltpu.VMEM((rows, ff), BF16),
        dma((9,)),
        dma((2, half + 1)), dma((2, half + 1)),
        dma((2, half + 1)), dma((2, half + 1)),
        dma((2, half + 1)), dma((2, half + 1)),
        dma((2, half + 1)), dma((2, half + 1)),
        dma((ny,)), dma((ny,)),
        dma((ny,)), dma((ny,)),
        dma((2, half + 1, 2)), dma((2, half + 1, 2)),
        dma((2, half + 1)), dma((2, half + 1)),
        dma((ngroup, ny)), dma((ngroup, ny)),
        dma((ny,)), dma((ny,)),
        dma((nt,)), dma((nt,)),
        dma((nt,)), dma((nt,)),
        dma((nt,)), dma((nt,)),
    ]
    return pl.pallas_call(
        functools.partial(layer_kernel, nz, ny, nt, rows, wrows, share),
        out_shape=jax.ShapeDtypeStruct((share, model), BF16),
        in_specs=[pl.BlockSpec(memory_space=pl.ANY)] * 9,
        out_specs=pl.BlockSpec(memory_space=pltpu.VMEM),
        scratch_shapes=scratch,
        compiler_params=pltpu.CompilerParams(
            collective_id=0, has_side_effects=True, vmem_limit_bytes=60 * 1024 * 1024
        ),
        name="layer",
    )(kv, off, q, gu, dt, stream, out_narrow, out_broad, gain)


def build(mesh, nz, ny, nt):
    torus = Mesh(mesh.devices.reshape(nz, ny, nt), SP_TP)
    in_specs = (
        P(SP, None),
        P(SP, "tp"),
        P(SP, "tp"),
        P(SP, "tp"),
        P(SP, "tp"),
        P(SP, "tp"),
        P(SP, "tp"),
        P(SP, "tp"),
        P("tp", None),
        P("tp", None),
        P(),
        P(SP, "tp"),
        P(SP, "tp"),
        P("tp", SP),
    )
    return jax.shard_map(
        functools.partial(local, nz, ny, nt),
        mesh=torus,
        in_specs=in_specs,
        out_specs=P(SP_TP, None),
        check_vma=False,
    )


def solution(mesh):
    sp = mesh.shape["sp"]
    ny = 4
    return build(mesh, sp // ny, ny, mesh.shape["tp"])
```

time: 435 us -> 110 us (0.25)
  blocking collectives: 146 us -> 0 us
  waiting for transfers between devices: 109 us -> 0 us
  Pallas kernels: 0 us -> 102 us
  matrix products: 93 us -> 0 us
  other arithmetic: 32.7 us -> 2.66 us
  starting transfers between devices: 19.2 us -> 0 us
  between operations: 13.7 us -> 0.05 us
  local copies, waits for them, and re-layouts: 17.6 us -> 4.47 us
    all_gather x7 -> x0, blocking collectives: 146 us -> none  [the longest x6 136 us: gather_in_order(): blocks = lax.all_gather(blocks, axes[k], axis=0, tiled=True)]
    pallas_call x0 -> x1, Pallas kernels: none -> 102 us  [local(): pl.pallas_call(functools.partial(layer_kernel, nz, ny, nt, rows, wrows, s...]
    dot_general x68 -> x0, matrix products: 93 us -> none  [the longest x32 46.6 us: weighted_values(): jnp.einsum('hqk,khd->qhd', weights, values, preferred_element_type=jnp.fl...]
    all_gather x6 -> x0, waiting for transfers between devices: 61.6 us -> none  [the longest x4 38.4 us: gather_in_order(): blocks = lax.all_gather(blocks, axes[k], axis=0, tiled=True)]
    all_to_all x2 -> x0, waiting for transfers between devices: 47.4 us -> none  [the longest x1 38.1 us: sent_to_all(): lax.all_to_all(jnp.broadcast_to(shard[None], (peers, *shard.shape)), axis...]
    another operation x64 -> x0, other arithmetic: 21.8 us -> none  [the longest x32 12.2 us: weighted_values(): within = lax.cumsum(grouped, axis=3, reverse=True) - grouped]
    all_to_all x2 -> x0, starting transfers between devices: 19 us -> none  [the longest x1 13.6 us: summed_on_arrival(): lax.all_to_all(cut_along(shard, dim, peers), axis, 0, 0, tiled=True)]
    reduce_sum x19 -> x0, other arithmetic: 9.01 us -> none  [the longest x16 5.7 us: back_step(): subs_broad.sum(axis=2)]
  transfers between devices with their start and end apart: 8 -> 0, of which waited for: 5 -> 0; matrix products, arithmetic and copies ran while one was open for 32% -> 0% of each run, Pallas kernels for 0% -> 0%
where the time goes in v1:
time: 110 us; the launch traced here: 109 us
  Pallas kernels  102 us (93%)
  local copies, waits for them, and re-layouts  4.47 us (4%)
  other arithmetic  2.66 us (2%)
    pallas_call x1, Pallas kernels, local(): pl.pallas_call(functools.partial(layer_kernel, nz, ny, nt, rows, wrows, s...  102 us
    unnamed x18, local copies, waits for them, and re-layouts  3.87 us

profile of v1, /device:TPU:1, one launch (start us, length us, event | category | flops | bytes accessed | tf_op | source)
XLA Modules:
  0.0 109.5 jit_solution(5653837802641617629)
XLA Ops:
  0.0 0.0 copy-start.2
  0.0 0.7 multiply_bitcast_fusion
  0.7 0.6 pad.8.off_in
  1.3 0.8 copy.17
  2.1 0.0 copy-done.2
  2.1 0.0 copy-start.5
  2.1 0.6 fusion.1.q_in
  2.8 0.1 copy-done.5
  2.8 0.0 copy-start.6
  2.8 0.0 copy-start.1
  2.9 0.1 copy.15
  3.0 0.6 copy-done.6
  3.6 0.0 copy-start
  3.6 0.1 copy.16
  3.7 0.0 copy-done.1
  3.7 0.6 copy-done
  4.3 0.0 copy-start.3
  4.3 0.0 copy-start.4
  4.3 0.7 pad_maximum_fusion.kv_in
  5.1 0.0 copy-done.3
  5.1 0.0 copy-done.4
  5.1 0.6 pad_maximum_fusion.1.gu_in
  5.7 102.3 %layer.1 = bf16[16,2048]{1,0:T(8,128)(2,1)} custom-call(bf16[384,128]{1,0:T(8,128)(2,1)} %pad_maximum_fusion.kv_in, f32[8,128]{1,0:T(8,128)} %pad.8.off_in, bf16[256,128]{1,0:T(8,128)(2,1)} %fusion.1.q_in, bf16[64,384]{1,0:T(8,128)(2,1)} %pad_maximum_fusion.1.gu_in, bf16[32,384]{1,0:T(8,128)(2,1)} %bitcast.4, bf16[128,2048]{1,0:T(8,128)(2,1)} %stream_in.1, ...), custom_call_target="tpu_custom_call" | custom-call | tf_op jit(solution)/shard_map/layer/pallas_call | solution.py:469
  108.0 1.5 %copy.19 = bf16[16,2048]{1,0:T(8,128)(2,1)} copy(bf16[16,2048]{1,0:T(8,128)(2,1)} %layer.1) | data formatting | bytes 131072
Async XLA Ops:
  0.0 2.1 %copy-start.2 = (bf16[128,128]{1,0:T(8,128)(2,1)S(1)}, bf16[128,128]{1,0:T(8,128)(2,1)}, u32[]{:S(2)}) copy-start(bf16[128,128]{1,0:T(8,128)(2,1)} %param.16) | copy-start | bytes 98308
  2.1 0.7 copy-start.5
  2.8 0.7 copy-start.6
  2.8 0.8 copy-start.1
  3.6 0.8 copy-start
  4.3 0.7 copy-start.3
  4.3 0.8 copy-start.4

commit v2 on v1

v2 whole, which is shorter than its diff:
```python
import functools
import math

import jax
import jax.numpy as jnp
from jax import lax
from jax.experimental import pallas as pl
from jax.experimental.pallas import tpu as pltpu
from jax.sharding import Mesh
from jax.sharding import PartitionSpec as P

NARROW_SIZE = 64
BROAD_SIZE = 128
SP = ("sp_0", "sp_1")
SP_TP = ("sp_0", "sp_1", "tp")
MESH = pl.DeviceIdType.MESH
LOG2E = 1.4426950408889634
SCALE = (NARROW_SIZE**-0.5 * LOG2E, BROAD_SIZE**-0.5 * LOG2E)
norm_eps = 1e-06
F32 = jnp.float32
BF16 = jnp.bfloat16
NT = (((1,), (1,)), ((), ()))
NN = (((1,), (0,)), ((), ()))


def dot(a, b, dims=NN, precision=None):
    return lax.dot_general(a, b, dims, preferred_element_type=F32, precision=precision)


def wrap(value, size):
    return lax.rem(value + 2 * size, size)


def layer_kernel(
    nz, ny, nt, rows, wrows, share,
    stream_in, qn_in, qb_in, kn_in, kb_in, vn_in, vb_in, off_in, on_in, ob_in, gain_in,
    gate_in, up_in, down_in,
    out,
    kv, off, qs, w, on, ob, st, gain, obuf, tall, ar, ao, part, rs, nb, mid_s, part2, rs2,
    qn, tcol, trow,
    lsem, kvs, kvr, offs, offr, ws, wr, q_s, q_r, yas, yar, yrs, yrr,
    t_s, t_r, a_s, a_r, r1s, r1r, n_s, n_r, r2s, r2r,
):
    z = lax.axis_index("sp_0")
    y = lax.axis_index("sp_1")
    t = lax.axis_index("tp")
    up = (wrap(z + 1, nz), y, t)
    dn = (wrap(z - 1, nz), y, t)
    yp = (z, wrap(y + 1, ny), t)
    ym = (z, wrap(y - 1, ny), t)
    half = nz // 2
    narrow = qn.shape[1]

    def ypeer(j):
        return (z, wrap(y + j, ny), t)

    def toff(j):
        core = lax.rem(t, 2)
        return wrap(t - core + 2 * (j // 2), nt) + (core + j % 2 - 2 * core * (j % 2))

    def tpeer(j):
        return (z, y, toff(j))

    far = sorted(range(1, nt), key=lambda j: -min(j // 2, (nt - j) // 2 if j % 2 == 0 else (nt + 1 - j) // 2))

    def rc(src, dst, ssem, rsem, dev):
        return pltpu.make_async_remote_copy(
            src_ref=src, dst_ref=dst, send_sem=ssem, recv_sem=rsem,
            device_id=dev, device_id_type=MESH,
        )

    barrier = pltpu.get_barrier_semaphore()
    peers = [up, dn] + [ypeer(j) for j in range(1, ny)] + [tpeer(j) for j in range(1, nt)]
    for p in peers:
        pl.semaphore_signal(barrier, inc=1, device_id=p, device_id_type=MESH)

    pairs = [
        (kn_in, kv.at[z, 0, pl.ds(0, narrow), :]),
        (vn_in, kv.at[z, 0, pl.ds(narrow, narrow), :]),
        (kb_in, kv.at[z, 1]),
        (vb_in, kv.at[z, 2]),
        (off_in, off.at[z]),
        (qn_in, qs.at[y, pl.ds(0, narrow), :]),
        (qb_in, qs.at[y, pl.ds(narrow, rows), :]),
        (gate_in, w.at[z, y, pl.ds(0, wrows), :]),
        (up_in, w.at[z, y, pl.ds(wrows, wrows), :]),
        (down_in, w.at[z, y, pl.ds(2 * wrows, wrows), :]),
        (stream_in.at[pl.ds(t * share, share), :], st),
        (on_in, on),
        (ob_in, ob),
        (gain_in, gain),
    ]
    copies = [pltpu.make_async_copy(a, b, lsem.at[i]) for i, (a, b) in enumerate(pairs)]
    first, second = copies[:10], copies[10:]
    for c in copies:
        c.start()

    tcol[...] = jnp.zeros(tcol.shape, F32)

    def zero_body(i, carry):
        obuf[i] = jnp.zeros(obuf.shape[1:], F32)
        return carry

    lax.fori_loop(0, nz, zero_body, 0)
    for c in first:
        c.wait()
    pl.semaphore_wait(barrier, len(peers))

    def shard_z(d, k):
        return wrap(z - k, nz) if d == 0 else wrap(z + k, nz)

    def ring(ref, ssem, rsem, d):
        return rc(ref, ref, ssem, rsem, up if d == 0 else dn)

    def kv_ring(d, k, c):
        return ring(kv.at[shard_z(d, k - 1), c], kvs.at[d, k, c], kvr.at[d, k, c], d)

    def off_ring(d, k):
        return ring(off.at[shard_z(d, k - 1)], offs.at[d, k], offr.at[d, k], d)

    def w_ring(d, k):
        return ring(w.at[shard_z(d, k - 1), y], ws.at[d, k], wr.at[d, k], d)

    def w_y(d, k, e):
        ref = w.at[shard_z(d, k), y]
        return rc(ref, ref, yas.at[d, k, e], yar.at[d, k, e], yp if e == 0 else ym)

    def w_relay(d, k):
        src_y = wrap(y - 1, ny) if d == 0 else wrap(y + 1, ny)
        ref = w.at[shard_z(d, k), src_y]
        return rc(ref, ref, yrs.at[d, k], yrr.at[d, k], yp if d == 0 else ym)

    def q_send(j):
        return rc(qs.at[y], qs.at[y], q_s.at[j], q_r.at[j], ypeer(j))

    def t_send(g, j):
        ref = tall.at[y, g]
        return rc(ref, ref, t_s.at[g, j], t_r.at[g, j], ypeer(j))

    for j in range(1, ny):
        q_send(j).start()
    for d in range(2):
        off_ring(d, 1).start()
    for c in range(3):
        for d in range(2):
            kv_ring(d, 1, c).start()
    for d in range(2):
        w_ring(d, 1).start()
    for e in range(2):
        w_y(0, 0, e).start()

    nq = ny * rows
    key_row = lax.broadcasted_iota(jnp.int32, (2 * rows, 2 * rows), 0)
    key_col = lax.broadcasted_iota(jnp.int32, (2 * rows, 2 * rows), 1)
    same_block = lax.div(key_row, rows) == lax.div(key_col, rows)
    tri = jnp.where(jnp.logical_and(key_row > key_col, same_block), 1.0, 0.0).astype(BF16)
    pick_row = lax.broadcasted_iota(jnp.int32, (2 * rows, 128), 0)
    pick_col = lax.broadcasted_iota(jnp.int32, (2 * rows, 128), 1)

    def process(blocks, h, diag):
        nk = len(blocks) * rows
        if h == 0:
            keys = [kv[zz, 0, 0:narrow, :] for zz, _, _ in blocks]
            logits = dot(qn[...], jnp.concatenate(keys, axis=1))
        else:
            keys = [kv[zz, 1] for zz, _, _ in blocks]
            logits = dot(qs[:, narrow:, :].reshape(nq, 128), jnp.concatenate(keys, axis=0), NT)
        bias = [off[zz, h : h + 1, :] * LOG2E for zz, _, _ in blocks]
        if not diag:
            bias = [jnp.where(b[2], v, -1e30) for b, v in zip(blocks, bias)]
        logits = logits * SCALE[h] + jnp.concatenate(bias, axis=1)
        soft = jnp.maximum(jnp.log2(1.0 + jnp.exp2(jnp.minimum(logits, 126.0))), logits)
        if diag:
            q_pos = lax.broadcasted_iota(jnp.int32, (nq, rows), 0)
            k_pos = y * rows + lax.broadcasted_iota(jnp.int32, (nq, rows), 1)
            causal = k_pos < q_pos
            low = jnp.where(causal, soft, 0.0).astype(BF16)
        else:
            low = soft.astype(BF16)
        place = 2 * blocks[0][1] + h
        if len(blocks) > 1:
            place = jnp.where(pick_row < rows, place, 2 * blocks[1][1] + h)
        pick = jnp.where(pick_col == place, 1.0, 0.0).astype(BF16)
        tcol[...] += dot(low, pick[0:nk])
        weight = jnp.exp2(logits - soft - dot(low, tri[0:nk, 0:nk]))
        if diag:
            weight = jnp.where(causal, weight, 0.0)
        weight = weight.astype(BF16)
        base = h * narrow
        for i, (zz, s, _) in enumerate(blocks):
            vt = kv[zz, 0, narrow:, :] if h == 0 else jnp.transpose(kv[zz, 2])
            obuf[s, base : base + vt.shape[0], :] = dot(
                vt, weight[:, i * rows : (i + 1) * rows], NT
            )

    def pass_on(make, k):
        for d in range(2):
            def one(d=d):
                make(d, k).wait_recv()

                @pl.when(k < half - d)
                def _():
                    make(d, k + 1).start()

            if d == 0:
                one()
            else:
                pl.when(k < half)(one)

    def forward(k):
        pass_on(off_ring, k)
        for c in range(3):
            pass_on(lambda d, kk, c=c: kv_ring(d, kk, c), k)

    def forward_w(k):
        pass_on(w_ring, k)
        for e in range(2):
            w_y(0, k, e).start()

        @pl.when(k < half)
        def _():
            for e in range(2):
                w_y(1, k, e).start()

    def forward_body(k, carry):
        forward(k)
        return carry

    lax.fori_loop(1, 3, forward_body, 0)
    forward_w(jnp.int32(1))
    for j in range(1, ny):
        q_send(j).wait_recv()
    for i in range(ny):
        head = jnp.transpose(qs[i, 0:narrow, :].astype(F32))
        qn[i * rows : (i + 1) * rows, :] = head.astype(BF16)
    for h in range(2):
        process([(z, jnp.int32(0), None)], h, True)

    def kv_step(k, carry):
        pl.when(k >= 3)(functools.partial(forward, k))
        blocks = [
            (wrap(z - k, nz), 2 * k - 1, k <= z),
            (wrap(z + k, nz), 2 * k, jnp.logical_and(k < half, z + k >= nz)),
        ]
        pl.when(k <= z)(functools.partial(process, blocks, 0, False))
        pl.when(k >= 3)(functools.partial(forward_w, k - 1))
        pl.when(k <= z)(functools.partial(process, blocks, 1, False))

        @pl.when(lax.rem(k, 2) == 0)
        def _():
            g = lax.div(k, 2) - 1
            trow[...] = jnp.transpose(tcol[...])
            tall[y, g] = trow[pl.ds(pl.multiple_of(8 * g, 8), 8), :]
            for j in range(1, ny):
                t_send(g, j).start()

        return carry

    lax.fori_loop(1, half + 1, kv_step, 0)

    ngroup = nz // 4
    for g in range(ngroup):
        for j in range(1, ny):
            t_send(g, j).wait_recv()

    trows = ny * ngroup * 8
    nrow = 2 * nz
    flat = tall[...].reshape(trows, nq)
    fr = lax.broadcasted_iota(jnp.int32, (nrow, trows), 0)
    fc = lax.broadcasted_iota(jnp.int32, (nrow, trows), 1)

    def slot_z(slot):
        k = lax.shift_right_logical(slot + 1, 1)
        signed = jnp.where(lax.bitwise_and(slot, 1) == 1, -k, k)
        return lax.bitwise_and(z + signed + nz, nz - 1)

    per_y = ngroup * 8
    c_y = lax.div(fc, per_y)
    c_in = lax.rem(fc, per_y)
    r_order = slot_z(lax.shift_right_logical(fr, 1)) * ny + y
    c_order = slot_z(lax.shift_right_logical(c_in, 1)) * ny + c_y
    same = lax.bitwise_and(fr, 1) == lax.bitwise_and(c_in, 1)
    sel = jnp.where(jnp.logical_and(same, c_order > r_order), 1.0, 0.0).astype(F32)
    later = dot(sel, flat, NN, lax.Precision.HIGHEST)
    factor = jnp.exp2(-later)
    for rb in range(ny):
        cols = slice(rb * rows, (rb + 1) * rows)
        for lo, hi, h in ((0, narrow, 0), (narrow, narrow + 128, 1)):
            acc = jnp.zeros((hi - lo, rows), F32)
            for s in range(nz):
                row = factor[2 * s + h : 2 * s + h + 1, cols]
                acc = acc + row * obuf[s, lo:hi, cols]
            ao[rb, lo:hi, :] = acc.astype(BF16)

    def a_send(j):
        peer = wrap(y + j, ny)
        return rc(ao.at[peer], ar.at[j], a_s.at[j], a_r.at[j], ypeer(j))

    for j in range(1, ny):
        a_send(j).start()
    forward_w(jnp.int32(half))
    for k in range(half):
        w_y(0, k, 0).wait_recv()
        w_relay(0, k).start()
        if k >= 1:
            w_y(1, k, 1).wait_recv()
            w_relay(1, k).start()
    for c in second:
        c.wait()
    attended = ao[y].astype(F32)
    for j in range(1, ny):
        a_send(j).wait_recv()
        attended = attended + ar[j].astype(F32)
    att_n = jnp.transpose(attended[0:narrow, :]).astype(BF16)
    att_b = jnp.transpose(attended[narrow : narrow + 128, :]).astype(BF16)
    model = out.shape[1]
    for c in range(model // 512):
        cols = slice(c * 512, (c + 1) * 512)
        block = (dot(att_n, on[:, cols]) + dot(att_b, ob[:, cols])).astype(BF16)
        part[:, :, cols] = block.reshape(nt, share, 512)

    def r1_send(j):
        return rc(part.at[toff(j)], rs.at[j], r1s.at[j], r1r.at[j], tpeer(j))

    for j in far:
        r1_send(j).start()
    w_y(0, half, 0).wait_recv()
    w_relay(0, half).start()
    total = st[...].astype(F32) + part[t].astype(F32)
    for j in range(1, nt):
        r1_send(j).wait_recv()
        total = total + rs[j].astype(F32)
    mid = total.astype(BF16).astype(F32)
    mid_s[...] = mid
    normed = mid * lax.rsqrt(jnp.mean(mid * mid, axis=1, keepdims=True) + norm_eps) * gain[...]
    nb[t] = normed.astype(BF16)

    def n_send(j):
        return rc(nb.at[t], nb.at[t], n_s.at[j], n_r.at[j], tpeer(j))

    for j in far:
        n_send(j).start()

    def w_wait(k, d):
        if d == 0:
            w_y(0, k, 1).wait_recv()
            w_relay(0, k).wait_recv()
        else:
            w_y(1, k, 0).wait_recv()
            w_relay(1, k).wait_recv()

    def w_wait_body(k, carry):
        w_wait(k, 0)

        @pl.when(jnp.logical_and(k >= 1, k < half))
        def _():
            w_wait(k, 1)

        return carry

    lax.fori_loop(0, half + 1, w_wait_body, 0)
    for j in range(1, nt):
        n_send(j).wait_recv()
    gate = jnp.zeros((rows, w.shape[3]), F32)
    upv = jnp.zeros((rows, w.shape[3]), F32)
    span = ny * wrows
    for zz in range(nz):
        lhs = nb[:, :, zz * span : (zz + 1) * span].reshape(rows, span)
        gate = gate + dot(lhs, w[zz, :, 0:wrows, :].reshape(span, w.shape[3]))
        upv = upv + dot(lhs, w[zz, :, wrows : 2 * wrows, :].reshape(span, w.shape[3]))
    hidden = (gate / (1.0 + jnp.exp(-gate)) * upv).astype(BF16)
    for zz in range(nz):
        rhs = w[zz, :, 2 * wrows :, :].reshape(span, w.shape[3])
        block = dot(hidden, rhs, NT).astype(BF16)
        part2[:, :, zz * span : (zz + 1) * span] = block.reshape(nt, share, span)

    def r2_send(j):
        return rc(part2.at[toff(j)], rs2.at[j], r2s.at[j], r2r.at[j], tpeer(j))

    for j in far:
        r2_send(j).start()

    def drain(k, carry):
        for d in range(2):
            @pl.when(k <= half - d)
            def _():
                for c in range(3):
                    kv_ring(d, k, c).wait_send()
                off_ring(d, k).wait_send()
                w_ring(d, k).wait_send()
                for e in range(2):
                    w_y(d, k, e).wait_send()
                w_relay(d, k).wait_send()
        return carry

    lax.fori_loop(1, half + 1, drain, 0)
    for e in range(2):
        w_y(0, 0, e).wait_send()
    w_relay(0, 0).wait_send()
    for j in range(1, ny):
        q_send(j).wait_send()
        a_send(j).wait_send()
        for g in range(ngroup):
            t_send(g, j).wait_send()
    for j in range(1, nt):
        r1_send(j).wait_send()
        n_send(j).wait_send()
    total = mid_s[...] + part2[t].astype(F32)
    for j in range(1, nt):
        r2_send(j).wait_recv()
        total = total + rs2[j].astype(F32)
    out[...] = total.astype(BF16)
    for j in range(1, nt):
        r2_send(j).wait_send()


def local(
    nz, ny, nt,
    stream, query_narrow, query_broad, key_narrow, key_broad, value_narrow, value_broad,
    key_offsets, out_narrow, out_broad, norm_gain, gate_weight, up_weight, down_weight,
):
    rows, model = stream.shape
    wrows, ff = gate_weight.shape
    share = rows // nt
    half = nz // 2
    ngroup = nz // 4
    gain = norm_gain.reshape(1, model)
    dma = pltpu.SemaphoreType.DMA
    scratch = [
        pltpu.VMEM((nz, 3, rows, 128), BF16),
        pltpu.VMEM((nz, 2, rows), F32),
        pltpu.VMEM((ny, 192, 128), BF16),
        pltpu.VMEM((nz, ny, 3 * wrows, ff), BF16),
        pltpu.VMEM((64, model), BF16),
        pltpu.VMEM((128, model), BF16),
        pltpu.VMEM((share, model), BF16),
        pltpu.VMEM((1, model), F32),
        pltpu.VMEM((nz + 1, 192, ny * rows), F32),
        pltpu.VMEM((ny, ngroup, 8, ny * rows), F32),
        pltpu.VMEM((ny, 192, rows), BF16),
        pltpu.VMEM((ny, 192, rows), BF16),
        pltpu.VMEM((nt, share, model), BF16),
        pltpu.VMEM((nt, share, model), BF16),
        pltpu.VMEM((nt, share, model), BF16),
        pltpu.VMEM((share, model), F32),
        pltpu.VMEM((nt, share, model), BF16),
        pltpu.VMEM((nt, share, model), BF16),
        pltpu.VMEM((ny * rows, 64), BF16),
        pltpu.VMEM((ny * rows, 128), F32),
        pltpu.VMEM((128, ny * rows), F32),
        dma((14,)),
        dma((2, half + 1, 3)), dma((2, half + 1, 3)),
        dma((2, half + 1)), dma((2, half + 1)),
        dma((2, half + 1)), dma((2, half + 1)),
        dma((ny,)), dma((ny,)),
        dma((2, half + 1, 2)), dma((2, half + 1, 2)),
        dma((2, half + 1)), dma((2, half + 1)),
        dma((ngroup, ny)), dma((ngroup, ny)),
        dma((ny,)), dma((ny,)),
        dma((nt,)), dma((nt,)),
        dma((nt,)), dma((nt,)),
        dma((nt,)), dma((nt,)),
    ]
    return pl.pallas_call(
        functools.partial(layer_kernel, nz, ny, nt, rows, wrows, share),
        out_shape=jax.ShapeDtypeStruct((share, model), BF16),
        in_specs=[pl.BlockSpec(memory_space=pl.ANY)] * 14,
        out_specs=pl.BlockSpec(memory_space=pltpu.VMEM),
        scratch_shapes=scratch,
        compiler_params=pltpu.CompilerParams(
            collective_id=0, has_side_effects=True, vmem_limit_bytes=60 * 1024 * 1024
        ),
        name="layer",
    )(
        stream, query_narrow.T, query_broad, key_narrow.T, key_broad, value_narrow.T, value_broad,
        key_offsets.T, out_narrow, out_broad, gain, gate_weight, up_weight, down_weight.T,
    )


def build(mesh, nz, ny, nt):
    torus = Mesh(mesh.devices.reshape(nz, ny, nt), SP_TP)
    in_specs = (
        P(SP, None),
        P(SP, "tp"),
        P(SP, "tp"),
        P(SP, "tp"),
        P(SP, "tp"),
        P(SP, "tp"),
        P(SP, "tp"),
        P(SP, "tp"),
        P("tp", None),
        P("tp", None),
        P(),
        P(SP, "tp"),
        P(SP, "tp"),
        P("tp", SP),
    )
    return jax.shard_map(
        functools.partial(local, nz, ny, nt),
        mesh=torus,
        in_specs=in_specs,
        out_specs=P(SP_TP, None),
        check_vma=False,
    )


def solution(mesh):
    sp = mesh.shape["sp"]
    ny = 4
    return build(mesh, sp // ny, ny, mesh.shape["tp"])
```

time: 110 us -> 90.2 us (0.82)
  Pallas kernels: 102 us -> 88.6 us
  local copies, waits for them, and re-layouts: 4.47 us -> 1.47 us
  other arithmetic: 2.66 us -> 0 us
    pallas_call x1, Pallas kernels: 102 us -> 88.6 us  [local(): pl.pallas_call(functools.partial(layer_kernel, nz, ny, nt, rows, wrows, s...]
    unnamed x18 -> x1, local copies, waits for them, and re-layouts: 3.87 us -> 1.47 us
    concatenate x3 -> x0, other arithmetic: 1.97 us -> none  [the longest x1 0.72 us: local(): jnp.concatenate([jnp.concatenate([key_narrow, value_narrow], axis=1), key...]
where the time goes in v2:
time: 90.2 us; the launch traced here: 90 us
  Pallas kernels  88.6 us (98%)
  local copies, waits for them, and re-layouts  1.47 us (2%)
    pallas_call x1, Pallas kernels, local(): pl.pallas_call(functools.partial(layer_kernel, nz, ny, nt, rows, wrows, s...  88.6 us

profile of v2, /device:TPU:1, one launch (start us, length us, event | category | flops | bytes accessed | tf_op | source)
XLA Modules:
  0.0 90.0 jit_solution(16620159453408738259)
XLA Ops:
  0.0 88.6 %layer.1 = bf16[16,2048]{1,0:T(8,128)(2,1)} custom-call(bf16[128,2048]{1,0:T(8,128)(2,1)} %stream_in.1, bf16[64,128]{1,0:T(8,128)(2,1)} %bitcast.7, bf16[128,128]{1,0:T(8,128)(2,1)} %qb_in.1, bf16[64,128]{1,0:T(8,128)(2,1)} %bitcast.8, bf16[128,128]{1,0:T(8,128)(2,1)} %kb_in.1, bf16[64,128]{1,0:T(8,128)(2,1)} %bitcast.9, bf16[128,128]{1,0:T(8,128)(2,1)} %vb_in.1, ...), custom_call_target="tpu_custom_call" | custom-call | tf_op jit(solution)/shard_map/layer/pallas_call | solution.py:464
  88.6 1.5 %copy.16 = bf16[16,2048]{1,0:T(8,128)(2,1)} copy(bf16[16,2048]{1,0:T(8,128)(2,1)} %layer.1) | data formatting | bytes 131072

commit v3 on v2

--- a/solution.py
+++ b/solution.py
@@ -36,10 +36,10 @@
     stream_in, qn_in, qb_in, kn_in, kb_in, vn_in, vb_in, off_in, on_in, ob_in, gain_in,
     gate_in, up_in, down_in,
     out,
-    kv, off, qs, w, on, ob, st, gain, obuf, tall, ar, ao, part, rs, nb, mid_s, part2, rs2,
-    qn, tcol, trow,
+    kv, off, qs, w, ow, st, gain, obuf, tall, ar, ao, att, nb, part2, rs2,
+    qn, tcol, trow, fac,
     lsem, kvs, kvr, offs, offr, ws, wr, q_s, q_r, yas, yar, yrs, yrr,
-    t_s, t_r, a_s, a_r, r1s, r1r, n_s, n_r, r2s, r2r,
+    t_s, t_r, a_s, a_r, ows, owr, n_s, n_r, r2s, r2r,
 ):
     z = lax.axis_index("sp_0")
     y = lax.axis_index("sp_1")
@@ -85,23 +85,16 @@
         (gate_in, w.at[z, y, pl.ds(0, wrows), :]),
         (up_in, w.at[z, y, pl.ds(wrows, wrows), :]),
         (down_in, w.at[z, y, pl.ds(2 * wrows, wrows), :]),
-        (stream_in.at[pl.ds(t * share, share), :], st),
-        (on_in, on),
-        (ob_in, ob),
+        (on_in, ow.at[t, pl.ds(0, narrow), :]),
+        (ob_in, ow.at[t, pl.ds(narrow, rows), :]),
+        (stream_in, st),
         (gain_in, gain),
     ]
     copies = [pltpu.make_async_copy(a, b, lsem.at[i]) for i, (a, b) in enumerate(pairs)]
-    first, second = copies[:10], copies[10:]
+    first, second, third = copies[:10], copies[10:12], copies[12:]
     for c in copies:
         c.start()
 
-    tcol[...] = jnp.zeros(tcol.shape, F32)
-
-    def zero_body(i, carry):
-        obuf[i] = jnp.zeros(obuf.shape[1:], F32)
-        return carry
-
-    lax.fori_loop(0, nz, zero_body, 0)
     for c in first:
         c.wait()
     pl.semaphore_wait(barrier, len(peers))
@@ -132,6 +125,20 @@
 
     def q_send(j):
         return rc(qs.at[y], qs.at[y], q_s.at[j], q_r.at[j], ypeer(j))
+
+    partner = toff(1)
+    xp, xm, xo = toff(2), toff(nt - 2), toff(nt // 2)
+    core = lax.rem(t, 2)
+    nx = nt // 2
+
+    def ow_send(i):
+        src, dst = (
+            (t, partner), (t, xp), (t, xm),
+            (xm, partner), (xp, partner),
+            (jnp.where(core == 0, xm, xp), jnp.where(core == 0, xp, xm)),
+            (xo, partner),
+        )[i]
+        return rc(ow.at[src], ow.at[src], ows.at[i], owr.at[i], (z, y, dst))
 
     def t_send(g, j):
         ref = tall.at[y, g]
@@ -148,7 +155,20 @@
         w_ring(d, 1).start()
     for e in range(2):
         w_y(0, 0, e).start()
-
+    for c in second:
+        c.wait()
+    if nx > 2:
+        ow_send(1).start()
+        ow_send(2).start()
+    ow_send(0).start()
+
+    tcol[...] = jnp.zeros(tcol.shape, F32)
+
+    def zero_body(i, carry):
+        obuf[i] = jnp.zeros(obuf.shape[1:], F32)
+        return carry
+
+    lax.fori_loop(0, nz + 1, zero_body, 0)
     nq = ny * rows
     key_row = lax.broadcasted_iota(jnp.int32, (2 * rows, 2 * rows), 0)
     key_col = lax.broadcasted_iota(jnp.int32, (2 * rows, 2 * rows), 1)
@@ -212,8 +232,7 @@
         for c in range(3):
             pass_on(lambda d, kk, c=c: kv_ring(d, kk, c), k)
 
-    def forward_w(k):
-        pass_on(w_ring, k)
+    def w_sides(k):
         for e in range(2):
             w_y(0, k, e).start()
 
@@ -222,12 +241,18 @@
             for e in range(2):
                 w_y(1, k, e).start()
 
+    def relay(d, k):
+        w_y(d, k, d).wait_recv()
+        w_relay(d, k).start()
+
     def forward_body(k, carry):
         forward(k)
         return carry
 
     lax.fori_loop(1, 3, forward_body, 0)
-    forward_w(jnp.int32(1))
+    pass_on(w_ring, jnp.int32(1))
+    w_sides(jnp.int32(1))
+    relay(0, 0)
     for j in range(1, ny):
         q_send(j).wait_recv()
     for i in range(ny):
@@ -243,7 +268,26 @@
             (wrap(z + k, nz), 2 * k, jnp.logical_and(k < half, z + k >= nz)),
         ]
         pl.when(k <= z)(functools.partial(process, blocks, 0, False))
-        pl.when(k >= 3)(functools.partial(forward_w, k - 1))
+
+        @pl.when(k >= 3)
+        def _():
+            pass_on(w_ring, k - 1)
+            pl.when(k < half)(functools.partial(w_sides, k - 1))
+
+        @pl.when(jnp.logical_and(k > 3, k < half))
+        def _():
+            relay(0, k - 3)
+            relay(1, k - 3)
+
+        if nx > 2:
+            @pl.when(k == half - 2)
+            def _():
+                ow_send(1).wait_recv()
+                ow_send(2).wait_recv()
+                ow_send(5).start()
+                ow_send(3).start()
+                ow_send(4).start()
+
         pl.when(k <= z)(functools.partial(process, blocks, 1, False))
 
         @pl.when(lax.rem(k, 2) == 0)
@@ -282,64 +326,71 @@
     same = lax.bitwise_and(fr, 1) == lax.bitwise_and(c_in, 1)
     sel = jnp.where(jnp.logical_and(same, c_order > r_order), 1.0, 0.0).astype(F32)
     later = dot(sel, flat, NN, lax.Precision.HIGHEST)
-    factor = jnp.exp2(-later)
-    for rb in range(ny):
-        cols = slice(rb * rows, (rb + 1) * rows)
+    fac[...] = jnp.exp2(-later)
+
+    def a_send(j):
+        peer = wrap(y + j, ny)
+        return rc(ao.at[peer], ar.at[j], a_s.at[j], a_r.at[j], ypeer(j))
+
+    for j in (2, 1, 3, 0) if ny > 2 else range(ny - 1, -1, -1):
+        rb = wrap(y + j, ny)
+        cols = pl.ds(pl.multiple_of(rb * rows, rows), rows)
         for lo, hi, h in ((0, narrow, 0), (narrow, narrow + 128, 1)):
             acc = jnp.zeros((hi - lo, rows), F32)
             for s in range(nz):
-                row = factor[2 * s + h : 2 * s + h + 1, cols]
-                acc = acc + row * obuf[s, lo:hi, cols]
+                acc = acc + fac[2 * s + h : 2 * s + h + 1, cols] * obuf[s, lo:hi, cols]
             ao[rb, lo:hi, :] = acc.astype(BF16)
-
-    def a_send(j):
-        peer = wrap(y + j, ny)
-        return rc(ao.at[peer], ar.at[j], a_s.at[j], a_r.at[j], ypeer(j))
-
-    for j in range(1, ny):
-        a_send(j).start()
-    forward_w(jnp.int32(half))
-    for k in range(half):
-        w_y(0, k, 0).wait_recv()
-        w_relay(0, k).start()
+        if j > 0:
+            a_send(j).start()
+    pass_on(w_ring, jnp.int32(half))
+    w_sides(jnp.int32(half - 1))
+    w_sides(jnp.int32(half))
+    early = max(half - 3, 1)
+    for k in range(early, half - 1):
+        relay(0, k)
         if k >= 1:
-            w_y(1, k, 1).wait_recv()
-            w_relay(1, k).start()
-    for c in second:
-        c.wait()
+            relay(1, k)
+    if nx > 2:
+        ow_send(5).wait_recv()
+        ow_send(6).start()
     attended = ao[y].astype(F32)
     for j in range(1, ny):
         a_send(j).wait_recv()
         attended = attended + ar[j].astype(F32)
-    att_n = jnp.transpose(attended[0:narrow, :]).astype(BF16)
-    att_b = jnp.transpose(attended[narrow : narrow + 128, :]).astype(BF16)
+    att[t] = attended.astype(BF16)
+
+    def n_send(j):
+        return rc(att.at[t], att.at[t], n_s.at[j], n_r.at[j], tpeer(j))
+
+    for j in far:
+        n_send(j).start()
+    relay(0, half - 1)
+    relay(1, half - 1)
+    relay(0, half)
+    for c in third:
+        c.wait()
+    ow_send(0).wait_recv()
+    if nx > 2:
+        for i in (3, 4, 6):
+            ow_send(i).wait_recv()
+    for j in range(1, nt):
+        n_send(j).wait_recv()
     model = out.shape[1]
+    square = jnp.zeros((rows, 1), F32)
+    heads = [jnp.transpose(att[i]) for i in range(nt)]
     for c in range(model // 512):
         cols = slice(c * 512, (c + 1) * 512)
-        block = (dot(att_n, on[:, cols]) + dot(att_b, ob[:, cols])).astype(BF16)
-        part[:, :, cols] = block.reshape(nt, share, 512)
-
-    def r1_send(j):
-        return rc(part.at[toff(j)], rs.at[j], r1s.at[j], r1r.at[j], tpeer(j))
-
-    for j in far:
-        r1_send(j).start()
-    w_y(0, half, 0).wait_recv()
-    w_relay(0, half).start()
-    total = st[...].astype(F32) + part[t].astype(F32)
-    for j in range(1, nt):
-        r1_send(j).wait_recv()
-        total = total + rs[j].astype(F32)
-    mid = total.astype(BF16).astype(F32)
-    mid_s[...] = mid
-    normed = mid * lax.rsqrt(jnp.mean(mid * mid, axis=1, keepdims=True) + norm_eps) * gain[...]
-    nb[t] = normed.astype(BF16)
-
-    def n_send(j):
-        return rc(nb.at[t], nb.at[t], n_s.at[j], n_r.at[j], tpeer(j))
-
-    for j in far:
-        n_send(j).start()
+        block = st[:, cols].astype(F32)
+        for i in range(nt):
+            block = block + dot(heads[i], ow[i, :, cols])
+        block = block.astype(BF16)
+        st[:, cols] = block
+        wide = block.astype(F32)
+        square = square + jnp.sum(wide * wide, axis=1, keepdims=True)
+    inverse = lax.rsqrt(square * (1.0 / model) + norm_eps)
+    for c in range(model // 512):
+        cols = slice(c * 512, (c + 1) * 512)
+        nb[:, cols] = (st[:, cols].astype(F32) * inverse * gain[:, cols]).astype(BF16)
 
     def w_wait(k, d):
         if d == 0:
@@ -359,26 +410,27 @@
         return carry
 
     lax.fori_loop(0, half + 1, w_wait_body, 0)
-    for j in range(1, nt):
-        n_send(j).wait_recv()
     gate = jnp.zeros((rows, w.shape[3]), F32)
     upv = jnp.zeros((rows, w.shape[3]), F32)
     span = ny * wrows
     for zz in range(nz):
-        lhs = nb[:, :, zz * span : (zz + 1) * span].reshape(rows, span)
+        lhs = nb[:, zz * span : (zz + 1) * span]
         gate = gate + dot(lhs, w[zz, :, 0:wrows, :].reshape(span, w.shape[3]))
         upv = upv + dot(lhs, w[zz, :, wrows : 2 * wrows, :].reshape(span, w.shape[3]))
     hidden = (gate / (1.0 + jnp.exp(-gate)) * upv).astype(BF16)
-    for zz in range(nz):
-        rhs = w[zz, :, 2 * wrows :, :].reshape(span, w.shape[3])
-        block = dot(hidden, rhs, NT).astype(BF16)
-        part2[:, :, zz * span : (zz + 1) * span] = block.reshape(nt, share, span)
-
-    def r2_send(j):
-        return rc(part2.at[toff(j)], rs2.at[j], r2s.at[j], r2r.at[j], tpeer(j))
-
-    for j in far:
-        r2_send(j).start()
+    def r2_send(hf, j):
+        return rc(
+            part2.at[hf, toff(j)], rs2.at[hf, j], r2s.at[hf, j], r2r.at[hf, j], tpeer(j)
+        )
+
+    for hf in range(2):
+        for i in range(nz // 2):
+            zz = hf * (nz // 2) + i
+            rhs = w[zz, :, 2 * wrows :, :].reshape(span, w.shape[3])
+            block = dot(hidden, rhs, NT).astype(BF16)
+            part2[hf, :, :, i * span : (i + 1) * span] = block.reshape(nt, share, span)
+        for j in far:
+            r2_send(hf, j).start()
 
     def drain(k, carry):
         for d in range(2):
@@ -403,15 +455,22 @@
         for g in range(ngroup):
             t_send(g, j).wait_send()
     for j in range(1, nt):
-        r1_send(j).wait_send()
         n_send(j).wait_send()
-    total = mid_s[...] + part2[t].astype(F32)
-    for j in range(1, nt):
-        r2_send(j).wait_recv()
-        total = total + rs2[j].astype(F32)
-    out[...] = total.astype(BF16)
-    for j in range(1, nt):
-        r2_send(j).wait_send()
+    ow_send(0).wait_send()
+    if nx > 2:
+        for i in range(1, 7):
+            ow_send(i).wait_send()
+    mine = pl.ds(pl.multiple_of(t * share, share), share)
+    for hf in range(2):
+        cols = slice(hf * model // 2, (hf + 1) * model // 2)
+        total = st[mine, cols].astype(F32) + part2[hf, t].astype(F32)
+        for j in range(1, nt):
+            r2_send(hf, j).wait_recv()
+            total = total + rs2[hf, j].astype(F32)
+        out[:, cols] = total.astype(BF16)
+    for hf in range(2):
+        for j in range(1, nt):
+            r2_send(hf, j).wait_send()
 
 
 def local(
@@ -431,23 +490,21 @@
         pltpu.VMEM((nz, 2, rows), F32),
         pltpu.VMEM((ny, 192, 128), BF16),
         pltpu.VMEM((nz, ny, 3 * wrows, ff), BF16),
-        pltpu.VMEM((64, model), BF16),
-        pltpu.VMEM((128, model), BF16),
-        pltpu.VMEM((share, model), BF16),
+        pltpu.VMEM((nt, 192, model), BF16),
+        pltpu.VMEM((rows, model), BF16),
         pltpu.VMEM((1, model), F32),
         pltpu.VMEM((nz + 1, 192, ny * rows), F32),
         pltpu.VMEM((ny, ngroup, 8, ny * rows), F32),
         pltpu.VMEM((ny, 192, rows), BF16),
         pltpu.VMEM((ny, 192, rows), BF16),
-        pltpu.VMEM((nt, share, model), BF16),
-        pltpu.VMEM((nt, share, model), BF16),
-        pltpu.VMEM((nt, share, model), BF16),
-        pltpu.VMEM((share, model), F32),
-        pltpu.VMEM((nt, share, model), BF16),
-        pltpu.VMEM((nt, share, model), BF16),
+        pltpu.VMEM((nt, 192, rows), BF16),
+        pltpu.VMEM((rows, model), BF16),
+        pltpu.VMEM((2, nt, share, model // 2), BF16),
+        pltpu.VMEM((2, nt, share, model // 2), BF16),
         pltpu.VMEM((ny * rows, 64), BF16),
         pltpu.VMEM((ny * rows, 128), F32),
         pltpu.VMEM((128, ny * rows), F32),
+        pltpu.VMEM((2 * nz, ny * rows), F32),
         dma((14,)),
         dma((2, half + 1, 3)), dma((2, half + 1, 3)),
         dma((2, half + 1)), dma((2, half + 1)),
@@ -457,9 +514,9 @@
         dma((2, half + 1)), dma((2, half + 1)),
         dma((ngroup, ny)), dma((ngroup, ny)),
         dma((ny,)), dma((ny,)),
+        dma((7,)), dma((7,)),
         dma((nt,)), dma((nt,)),
-        dma((nt,)), dma((nt,)),
-        dma((nt,)), dma((nt,)),
+        dma((2, nt)), dma((2, nt)),
     ]
     return pl.pallas_call(
         functools.partial(layer_kernel, nz, ny, nt, rows, wrows, share),

time: 90.2 us -> 82 us (0.909)
  Pallas kernels: 88.6 us -> 80.3 us
    pallas_call x1, Pallas kernels: 88.6 us -> 80.3 us  [local(): pl.pallas_call(functools.partial(layer_kernel, nz, ny, nt, rows, wrows, s...]
where the time goes in v3:
time: 82 us; the launch traced here: 81.8 us
  Pallas kernels  80.3 us (98%)
  local copies, waits for them, and re-layouts  1.47 us (2%)
    pallas_call x1, Pallas kernels, local(): pl.pallas_call(functools.partial(layer_kernel, nz, ny, nt, rows, wrows, s...  80.3 us

profile of v3, /device:TPU:1, one launch (start us, length us, event | category | flops | bytes accessed | tf_op | source)
XLA Modules:
  0.0 81.8 jit_solution(6966139737597388713)
XLA Ops:
  0.0 80.3 %layer.1 = bf16[16,2048]{1,0:T(8,128)(2,1)} custom-call(bf16[128,2048]{1,0:T(8,128)(2,1)} %stream_in.1, bf16[64,128]{1,0:T(8,128)(2,1)} %bitcast.7, bf16[128,128]{1,0:T(8,128)(2,1)} %qb_in.1, bf16[64,128]{1,0:T(8,128)(2,1)} %bitcast.8, bf16[128,128]{1,0:T(8,128)(2,1)} %kb_in.1, bf16[64,128]{1,0:T(8,128)(2,1)} %bitcast.9, bf16[128,128]{1,0:T(8,128)(2,1)} %vb_in.1, ...), custom_call_target="tpu_custom_call" | custom-call | tf_op jit(solution)/shard_map/layer/pallas_call | solution.py:521
  80.3 1.5 %copy.16 = bf16[16,2048]{1,0:T(8,128)(2,1)} copy(bf16[16,2048]{1,0:T(8,128)(2,1)} %layer.1) | data formatting | bytes 131072

commit v4 on v3

--- a/solution.py
+++ b/solution.py
@@ -37,7 +37,7 @@
     gate_in, up_in, down_in,
     out,
     kv, off, qs, w, ow, st, gain, obuf, tall, ar, ao, att, nb, part2, rs2,
-    qn, tcol, trow, fac,
+    qn, tcol, trow, fac, acc, lowb, gap,
     lsem, kvs, kvr, offs, offr, ws, wr, q_s, q_r, yas, yar, yrs, yrr,
     t_s, t_r, a_s, a_r, ows, owr, n_s, n_r, r2s, r2r,
 ):
@@ -177,7 +177,7 @@
     pick_row = lax.broadcasted_iota(jnp.int32, (2 * rows, 128), 0)
     pick_col = lax.broadcasted_iota(jnp.int32, (2 * rows, 128), 1)
 
-    def process(blocks, h, diag):
+    def totals(blocks, h, diag):
         nk = len(blocks) * rows
         if h == 0:
             keys = [kv[zz, 0, 0:narrow, :] for zz, _, _ in blocks]
@@ -202,9 +202,15 @@
             place = jnp.where(pick_row < rows, place, 2 * blocks[1][1] + h)
         pick = jnp.where(pick_col == place, 1.0, 0.0).astype(BF16)
         tcol[...] += dot(low, pick[0:nk])
-        weight = jnp.exp2(logits - soft - dot(low, tri[0:nk, 0:nk]))
+        rest = logits - soft
         if diag:
-            weight = jnp.where(causal, weight, 0.0)
+            rest = jnp.where(causal, rest, -1e30)
+        lowb[h, :, 0:nk] = low
+        gap[h, :, 0:nk] = rest
+
+    def outputs(blocks, h):
+        nk = len(blocks) * rows
+        weight = jnp.exp2(gap[h, :, 0:nk] - dot(lowb[h, :, 0:nk], tri[0:nk, 0:nk]))
         weight = weight.astype(BF16)
         base = h * narrow
         for i, (zz, s, _) in enumerate(blocks):
@@ -252,14 +258,17 @@
     lax.fori_loop(1, 3, forward_body, 0)
     pass_on(w_ring, jnp.int32(1))
     w_sides(jnp.int32(1))
-    relay(0, 0)
+    w_y(0, 0, 1).wait_recv()
+    w_relay(1, 0).start()
     for j in range(1, ny):
         q_send(j).wait_recv()
     for i in range(ny):
         head = jnp.transpose(qs[i, 0:narrow, :].astype(F32))
         qn[i * rows : (i + 1) * rows, :] = head.astype(BF16)
     for h in range(2):
-        process([(z, jnp.int32(0), None)], h, True)
+        totals([(z, jnp.int32(0), None)], h, True)
+    for h in range(2):
+        outputs([(z, jnp.int32(0), None)], h)
 
     def kv_step(k, carry):
         pl.when(k >= 3)(functools.partial(forward, k))
@@ -267,14 +276,31 @@
             (wrap(z - k, nz), 2 * k - 1, k <= z),
             (wrap(z + k, nz), 2 * k, jnp.logical_and(k < half, z + k >= nz)),
         ]
-        pl.when(k <= z)(functools.partial(process, blocks, 0, False))
+
+        def both_totals():
+            totals(blocks, 0, False)
+            totals(blocks, 1, False)
+
+        def both_outputs():
+            outputs(blocks, 0)
+            outputs(blocks, 1)
+
+        pl.when(k <= z)(both_totals)
+
+        @pl.when(lax.rem(k, 2) == 0)
+        def _():
+            g = lax.div(k, 2) - 1
+            trow[...] = jnp.transpose(tcol[...])
+            tall[y, g] = trow[pl.ds(pl.multiple_of(8 * g, 8), 8), :]
+            for j in range(1, ny):
+                t_send(g, j).start()
 
         @pl.when(k >= 3)
         def _():
             pass_on(w_ring, k - 1)
             pl.when(k < half)(functools.partial(w_sides, k - 1))
 
-        @pl.when(jnp.logical_and(k > 3, k < half))
+        @pl.when(jnp.logical_and(k > 3, k < half - 1))
         def _():
             relay(0, k - 3)
             relay(1, k - 3)
@@ -288,16 +314,7 @@
                 ow_send(3).start()
                 ow_send(4).start()
 
-        pl.when(k <= z)(functools.partial(process, blocks, 1, False))
-
-        @pl.when(lax.rem(k, 2) == 0)
-        def _():
-            g = lax.div(k, 2) - 1
-            trow[...] = jnp.transpose(tcol[...])
-            tall[y, g] = trow[pl.ds(pl.multiple_of(8 * g, 8), 8), :]
-            for j in range(1, ny):
-                t_send(g, j).start()
-
+        pl.when(k <= z)(both_outputs)
         return carry
 
     lax.fori_loop(1, half + 1, kv_step, 0)
@@ -336,16 +353,16 @@
         rb = wrap(y + j, ny)
         cols = pl.ds(pl.multiple_of(rb * rows, rows), rows)
         for lo, hi, h in ((0, narrow, 0), (narrow, narrow + 128, 1)):
-            acc = jnp.zeros((hi - lo, rows), F32)
+            part = jnp.zeros((hi - lo, rows), F32)
             for s in range(nz):
-                acc = acc + fac[2 * s + h : 2 * s + h + 1, cols] * obuf[s, lo:hi, cols]
-            ao[rb, lo:hi, :] = acc.astype(BF16)
+                part = part + fac[2 * s + h : 2 * s + h + 1, cols] * obuf[s, lo:hi, cols]
+            ao[rb, lo:hi, :] = part.astype(BF16)
         if j > 0:
             a_send(j).start()
     pass_on(w_ring, jnp.int32(half))
     w_sides(jnp.int32(half - 1))
     w_sides(jnp.int32(half))
-    early = max(half - 3, 1)
+    early = max(half - 4, 1)
     for k in range(early, half - 1):
         relay(0, k)
         if k >= 1:
@@ -369,21 +386,28 @@
     relay(0, half)
     for c in third:
         c.wait()
-    ow_send(0).wait_recv()
     if nx > 2:
         for i in (3, 4, 6):
             ow_send(i).wait_recv()
-    for j in range(1, nt):
+    model = out.shape[1]
+
+    def project(i, head, first):
+        for c in range(model // 512):
+            cols = slice(c * 512, (c + 1) * 512)
+            base = st[:, cols].astype(F32) if first else acc[:, cols]
+            acc[:, cols] = base + dot(head, ow[i, :, cols])
+
+    project(t, jnp.transpose(att[t]), True)
+    for j in sorted(range(1, nt), key=lambda j: (min(j // 2, nt // 2 - j // 2), j)):
         n_send(j).wait_recv()
-    model = out.shape[1]
+        if j == 1:
+            ow_send(0).wait_recv()
+        i = toff(2 * ((nt // 2 - j // 2) % (nt // 2)) + j % 2)
+        project(i, jnp.transpose(att[i]), False)
     square = jnp.zeros((rows, 1), F32)
-    heads = [jnp.transpose(att[i]) for i in range(nt)]
     for c in range(model // 512):
         cols = slice(c * 512, (c + 1) * 512)
-        block = st[:, cols].astype(F32)
-        for i in range(nt):
-            block = block + dot(heads[i], ow[i, :, cols])
-        block = block.astype(BF16)
+        block = acc[:, cols].astype(BF16)
         st[:, cols] = block
         wide = block.astype(F32)
         square = square + jnp.sum(wide * wide, axis=1, keepdims=True)
@@ -392,6 +416,9 @@
         cols = slice(c * 512, (c + 1) * 512)
         nb[:, cols] = (st[:, cols].astype(F32) * inverse * gain[:, cols]).astype(BF16)
 
+    w_y(0, 0, 0).wait_recv()
+    w_relay(1, 0).wait_recv()
+
     def w_wait(k, d):
         if d == 0:
             w_y(0, k, 1).wait_recv()
@@ -403,13 +430,13 @@
     def w_wait_body(k, carry):
         w_wait(k, 0)
 
-        @pl.when(jnp.logical_and(k >= 1, k < half))
+        @pl.when(k < half)
         def _():
             w_wait(k, 1)
 
         return carry
 
-    lax.fori_loop(0, half + 1, w_wait_body, 0)
+    lax.fori_loop(1, half + 1, w_wait_body, 0)
     gate = jnp.zeros((rows, w.shape[3]), F32)
     upv = jnp.zeros((rows, w.shape[3]), F32)
     span = ny * wrows
@@ -448,7 +475,7 @@
     lax.fori_loop(1, half + 1, drain, 0)
     for e in range(2):
         w_y(0, 0, e).wait_send()
-    w_relay(0, 0).wait_send()
+    w_relay(1, 0).wait_send()
     for j in range(1, ny):
         q_send(j).wait_send()
         a_send(j).wait_send()
@@ -505,6 +532,9 @@
         pltpu.VMEM((ny * rows, 128), F32),
         pltpu.VMEM((128, ny * rows), F32),
         pltpu.VMEM((2 * nz, ny * rows), F32),
+        pltpu.VMEM((rows, model), F32),
+        pltpu.VMEM((2, ny * rows, 2 * rows), BF16),
+        pltpu.VMEM((2, ny * rows, 2 * rows), F32),
         dma((14,)),
         dma((2, half + 1, 3)), dma((2, half + 1, 3)),
         dma((2, half + 1)), dma((2, half + 1)),

time: 82 us -> 79.9 us (0.974)
  Pallas kernels: 80.3 us -> 78.2 us
    pallas_call x1, Pallas kernels: 80.3 us -> 78.2 us  [local(): pl.pallas_call(functools.partial(layer_kernel, nz, ny, nt, rows, wrows, s...]
where the time goes in v4:
time: 79.9 us; the launch traced here: 79.7 us
  Pallas kernels  78.2 us (98%)
  local copies, waits for them, and re-layouts  1.47 us (2%)
    pallas_call x1, Pallas kernels, local(): pl.pallas_call(functools.partial(layer_kernel, nz, ny, nt, rows, wrows, s...  78.2 us

profile of v4, /device:TPU:1, one launch (start us, length us, event | category | flops | bytes accessed | tf_op | source)
XLA Modules:
  0.0 79.7 jit_solution(8947210640267779808)
XLA Ops:
  0.0 78.2 %layer.1 = bf16[16,2048]{1,0:T(8,128)(2,1)} custom-call(bf16[128,2048]{1,0:T(8,128)(2,1)} %stream_in.1, bf16[64,128]{1,0:T(8,128)(2,1)} %bitcast.7, bf16[128,128]{1,0:T(8,128)(2,1)} %qb_in.1, bf16[64,128]{1,0:T(8,128)(2,1)} %bitcast.8, bf16[128,128]{1,0:T(8,128)(2,1)} %kb_in.1, bf16[64,128]{1,0:T(8,128)(2,1)} %bitcast.9, bf16[128,128]{1,0:T(8,128)(2,1)} %vb_in.1, ...), custom_call_target="tpu_custom_call" | custom-call | tf_op jit(solution)/shard_map/layer/pallas_call | solution.py:551
  78.2 1.5 %copy.16 = bf16[16,2048]{1,0:T(8,128)(2,1)} copy(bf16[16,2048]{1,0:T(8,128)(2,1)} %layer.1) | data formatting | bytes 131072

commit v5 on v4

--- a/solution.py
+++ b/solution.py
@@ -251,15 +251,12 @@
         w_y(d, k, d).wait_recv()
         w_relay(d, k).start()
 
-    def forward_body(k, carry):
-        forward(k)
-        return carry
-
-    lax.fori_loop(1, 3, forward_body, 0)
+    forward(jnp.int32(1))
     pass_on(w_ring, jnp.int32(1))
     w_sides(jnp.int32(1))
     w_y(0, 0, 1).wait_recv()
     w_relay(1, 0).start()
+    forward(jnp.int32(2))
     for j in range(1, ny):
         q_send(j).wait_recv()
     for i in range(ny):
@@ -295,12 +292,12 @@
             for j in range(1, ny):
                 t_send(g, j).start()
 
-        @pl.when(k >= 3)
+        @pl.when(jnp.logical_and(k >= 2, k < half))
         def _():
-            pass_on(w_ring, k - 1)
-            pl.when(k < half)(functools.partial(w_sides, k - 1))
-
-        @pl.when(jnp.logical_and(k > 3, k < half - 1))
+            pass_on(w_ring, k)
+            w_sides(k)
+
+        @pl.when(jnp.logical_and(k > 3, k < half - 2))
         def _():
             relay(0, k - 3)
             relay(1, k - 3)
@@ -360,9 +357,8 @@
         if j > 0:
             a_send(j).start()
     pass_on(w_ring, jnp.int32(half))
-    w_sides(jnp.int32(half - 1))
     w_sides(jnp.int32(half))
-    early = max(half - 4, 1)
+    early = max(half - 5, 1)
     for k in range(early, half - 1):
         relay(0, k)
         if k >= 1:

time: 79.9 us -> 79.2 us (level)
  no operation moved by 1% of the time
where the time goes in v5:
time: 79.2 us; the launch traced here: 79 us
  Pallas kernels  77.5 us (98%)
  local copies, waits for them, and re-layouts  1.47 us (2%)
    pallas_call x1, Pallas kernels, local(): pl.pallas_call(functools.partial(layer_kernel, nz, ny, nt, rows, wrows, s...  77.5 us

profile of v5, /device:TPU:1, one launch (start us, length us, event | category | flops | bytes accessed | tf_op | source)
XLA Modules:
  0.0 79.0 jit_solution(413957685086264331)
XLA Ops:
  0.0 77.5 %layer.1 = bf16[16,2048]{1,0:T(8,128)(2,1)} custom-call(bf16[128,2048]{1,0:T(8,128)(2,1)} %stream_in.1, bf16[64,128]{1,0:T(8,128)(2,1)} %bitcast.7, bf16[128,128]{1,0:T(8,128)(2,1)} %qb_in.1, bf16[64,128]{1,0:T(8,128)(2,1)} %bitcast.8, bf16[128,128]{1,0:T(8,128)(2,1)} %kb_in.1, bf16[64,128]{1,0:T(8,128)(2,1)} %bitcast.9, bf16[128,128]{1,0:T(8,128)(2,1)} %vb_in.1, ...), custom_call_target="tpu_custom_call" | custom-call | tf_op jit(solution)/shard_map/layer/pallas_call | solution.py:547
  77.5 1.5 %copy.16 = bf16[16,2048]{1,0:T(8,128)(2,1)} copy(bf16[16,2048]{1,0:T(8,128)(2,1)} %layer.1) | data formatting | bytes 131072
